TPU v7x, 512 devices: a whole 4x4x16 slice. The times are simulated.
512 devices in a mesh: ra: 16 (over z), cb: 4 (over y), dp: 8 (over x, core).
Axes of the slice: x: 4, y: 4, z: 16, core: 2. Of those that a mesh axis runs over, the one named last changes fastest.
Arguments:
- tokens: bfloat16 [8, 512, 4096], P('dp', None, 'ra'), may hold values from -80 to 80
- pre_gain: float32 [4096], P('ra'), may hold values from 0.1 to 1.9
- w_gate: bfloat16 [4096, 11264], P('ra', 'cb'), may hold values from -0.09375 to 0.09375
- w_up: bfloat16 [4096, 11264], P('ra', 'cb'), may hold values from -0.09375 to 0.09375
- conv_gate: float32 [3, 11264], P(None, 'cb'), may hold values from -3.5 to 3.5
- conv_up: float32 [3, 11264], P(None, 'cb'), may hold values from -3.5 to 3.5
- w_down: bfloat16 [11264, 4096], P('cb', 'ra'), may hold values from -2 to 2
- post_gain: float32 [4096], P('ra'), may hold values from 0.1 to 1.9
Outputs:
- mixed: bfloat16 [8, 512, 4096], P('dp', None, 'ra')
All inputs are finite; a program needn't handle non-finite values.
Results may differ from a plain program's by a relative error of at most 0.0064.
Values may be sent and summed in bfloat16 or wider, within the bound.
A program may use at most 64 MiB of HBM per device.

v0:
```python
import jax
import jax.numpy as jnp
from jax import lax
from jax.sharding import PartitionSpec as P

epsilon = 1e-06
residual_scale = 0.125


def from_everyone(array, axis):
    count = lax.axis_size(axis)
    return lax.all_to_all(
        jnp.broadcast_to(array[None], (count, *array.shape)), axis, 0, 0, tiled=True
    )


def over_copies(array, axis):
    return from_everyone(array, axis).sum(axis=0)


def split_up(array, dim, count):
    dims = array.shape
    tiles = array.reshape(*dims[:dim], count, dims[dim] // count, *dims[dim + 1 :])
    return jnp.moveaxis(tiles, dim, 0)


def summed_on_arrival(array, axis, dim):
    count = lax.axis_size(axis)
    tiles = lax.all_to_all(split_up(array, dim, count), axis, 0, 0, tiled=True)
    return jnp.sum(tiles, axis=0)


def convolve(field, tap_weights):
    zero_col = jnp.zeros((field.shape[0], 1), jnp.float32)
    before = jnp.concatenate([zero_col, field[:, :-1]], axis=1)
    later_cols = jnp.concatenate([field[:, 1:], zero_col], axis=1)
    return (
        tap_weights[0][:, None] * before
        + tap_weights[1][:, None] * field
        + tap_weights[2][:, None] * later_cols
    )


def local(tokens, pre_gain, w_gate, w_up, conv_gate, conv_up, w_down, post_gain):
    ra_count = lax.axis_size("ra")
    dim_full = tokens.shape[2] * ra_count
    values = tokens[0].astype(jnp.float32)
    local_sq = jnp.sum(values * values, axis=1)
    total_sq = over_copies(local_sq, "ra")
    in_scale = lax.rsqrt(total_sq / dim_full + epsilon)
    weighted = (values * pre_gain).astype(jnp.bfloat16)
    gate_cols, up_cols = (
        lax.all_to_all(w_gate, "ra", split_axis=1, concat_axis=0, tiled=True),
        lax.all_to_all(w_up, "ra", split_axis=1, concat_axis=0, tiled=True),
    )
    own_units = gate_cols.shape[1]
    piece = lax.all_gather(weighted, "ra", axis=1, tiled=True)
    dims = (((0,), (1,)), ((), ()))
    gate_sum = lax.dot_general(gate_cols, piece, dims, preferred_element_type=jnp.float32)
    up_sum = lax.dot_general(up_cols, piece, dims, preferred_element_type=jnp.float32)
    offset_units = lax.axis_index("ra") * own_units
    taps_gate = lax.dynamic_slice_in_dim(conv_gate, offset_units, own_units, 1)
    taps_up = lax.dynamic_slice_in_dim(conv_up, offset_units, own_units, 1)
    gate_lin = gate_sum * in_scale[None, :]
    up_lin = up_sum * in_scale[None, :]
    hidden = (
        jax.nn.gelu(convolve(gate_lin, taps_gate), approximate=True) * convolve(up_lin, taps_up)
    ).astype(jnp.bfloat16)
    partial_value = lax.dot_general(
        lax.all_gather(hidden, "ra", axis=0, tiled=True),
        w_down,
        (((0,), (0,)), ((), ())),
        preferred_element_type=jnp.float32,
    )
    share = summed_on_arrival(partial_value, "cb", 1)
    share_cols = share.shape[1]
    col_start = lax.axis_index("cb") * share_cols
    own_values = lax.dynamic_slice_in_dim(values, col_start, share_cols, 1)
    own_gain = lax.dynamic_slice_in_dim(post_gain, col_start, share_cols, 0)
    post_sq = over_copies(jnp.sum(share * share, axis=1), ("ra", "cb"))
    post_scale = lax.rsqrt(post_sq / dim_full + epsilon)
    mixed_part = (residual_scale * own_values + share * post_scale[:, None] * own_gain).astype(
        jnp.bfloat16
    )
    mixed = lax.all_gather(mixed_part, "cb", axis=1, tiled=True)
    return mixed[None]


def solution(mesh):
    in_specs = (
        P("dp", None, "ra"),
        P("ra"),
        P("ra", "cb"),
        P("ra", "cb"),
        P(None, "cb"),
        P(None, "cb"),
        P("cb", "ra"),
        P("ra"),
    )
    out_specs = P("dp", None, "ra")
    return jax.shard_map(local, mesh=mesh, in_specs=in_specs, out_specs=out_specs, check_vma=False)
```

profile of v0, /device:TPU:6, one launch (start us, length us, event | category | flops | bytes accessed | tf_op | source)
XLA Modules:
  0.0 356.8 jit_solution(16461781965745227600)
XLA Ops:
  6.5 0.0 copy-start
  6.5 1.2 copy.25
  7.7 1.5 fusion.3
  9.2 0.6 broadcast_in_dim.6
  9.9 15.2 %all-to-all-start.1 = ((f32[16,1,512]{2,1,0:T(1,128)}), f32[16,1,512]{2,1,0:T(1,128)S(1)}, u32[]{:S(2)}, u32[]{:S(2)}) async-start(f32[16,1,512]{2,1,0:T(1,128)} %broadcast_in_dim.6), calls=%async_computation.1 | async-start | bytes 65536 | tf_op jit(solution)/shard_map/all_to_all | solution.py:12
  25.1 2.5 copy.29
  27.6 10.0 %all-to-all-done.1 = f32[16,1,512]{2,1,0:T(1,128)S(1)} async-done(((f32[16,1,512]{2,1,0:T(1,128)}), f32[16,1,512]{2,1,0:T(1,128)S(1)}, u32[]{:S(2)}, u32[]{:S(2)}) %all-to-all-start.1) | async-done | bytes 32800 | tf_op jit(solution)/shard_map/all_to_all | solution.py:12
  37.6 3.7 %all-to-all-start.2 = ((bf16[256,16,176]{0,2,1:T(8,128)(2,1)}), bf16[256,16,176]{0,2,1:T(8,128)(2,1)S(1)}, u32[]{:S(2)}, u32[]{:S(2)}) async-start(bf16[256,16,176]{0,2,1:T(8,128)(2,1)} %bitcast.41), calls=%async_computation.2 | async-start | bytes 2883584 | tf_op jit(solution)/shard_map/all_to_all | solution.py:54
  41.3 0.0 all-gather.3.cloned.1.call-start
  41.4 0.7 all-gather.3.cloned.1.call-update
  42.1 2.5 copy.26
  44.6 72.1 %all-to-all-done.2 = bf16[256,16,176]{0,2,1:T(8,128)(2,1)S(1)} async-done(((bf16[256,16,176]{0,2,1:T(8,128)(2,1)}), bf16[256,16,176]{0,2,1:T(8,128)(2,1)S(1)}, u32[]{:S(2)}, u32[]{:S(2)}) %all-to-all-start.2) | async-done | bytes 1441824 | tf_op jit(solution)/shard_map/all_to_all | solution.py:54
  116.7 10.3 %all-to-all-start = ((bf16[256,16,176]{0,2,1:T(8,128)(2,1)}), bf16[256,16,176]{0,2,1:T(8,128)(2,1)}, u32[]{:S(2)}, u32[]{:S(2)}) async-start(bf16[256,16,176]{0,2,1:T(8,128)(2,1)} %bitcast.40), calls=%async_computation | async-start | bytes 2883584 | tf_op jit(solution)/shard_map/all_to_all | solution.py:53
  127.0 0.0 all-gather.5.cloned.1.call-start
  127.1 0.9 constant_dynamic-slice_fusion
  128.0 1.3 copy.36
  129.3 78.8 %all-to-all-done = bf16[256,16,176]{0,2,1:T(8,128)(2,1)} async-done(((bf16[256,16,176]{0,2,1:T(8,128)(2,1)}), bf16[256,16,176]{0,2,1:T(8,128)(2,1)}, u32[]{:S(2)}, u32[]{:S(2)}) %all-to-all-start) | async-done | bytes 1441824 | tf_op jit(solution)/shard_map/all_to_all | solution.py:53
  208.2 0.0 copy-start.2
  208.2 2.8 copy.35
  210.9 5.6 %all-gather.3.cloned.1.call-done = bf16[512,4096]{0,1:T(8,128)(2,1)} async-done(((bf16[512,256]{0,1:T(8,128)(2,1)}), bf16[512,4096]{0,1:T(8,128)(2,1)}) %all-gather.3.cloned.1.call-update) | async-done | bytes 4194320 | tf_op jit(solution)/shard_map/all_gather | solution.py:57
  216.5 0.0 copy-done.2
  216.5 0.0 copy-start.1
  216.5 0.0 copy-start.3
  216.5 3.3 fusion.1
  219.8 0.2 copy-done.1
  220.0 0.4 copy-done.3
  220.4 0.9 fusion
  221.3 0.3 fusion.14
  221.6 1.2 fusion.12
  222.8 0.0 all-gather.5.cloned.1.call-update
  222.8 72.5 %all-gather.5.cloned.1.call-done = bf16[2816,512]{1,0:T(8,128)(2,1)} async-done(((bf16[176,512]{1,0:T(8,128)(2,1)}), bf16[2816,512]{1,0:T(8,128)(2,1)}) %all-gather.5.cloned.1.call-update) | async-done | bytes 2883600 | tf_op jit(solution)/shard_map/all_gather | solution.py:70
  295.4 0.0 copy-done
  295.4 2.8 fusion.16
  298.1 0.0 copy-start.4
  298.2 12.1 %all_to_all.55 = f32[4,512,64]{1,2,0:T(8,128)S(1)} all-to-all(f32[4,512,64]{1,2,0:T(8,128)S(1)} %bitcast.45), channel_id=1, replica_groups=mesh['ra'=16,'cb'=4,'dp'=8] {'cb'}, dimensions={0} | all-to-all | bytes 1048576 | tf_op jit(solution)/shard_map/all_to_all | solution.py:29
  310.3 0.7 broadcast_in_dim.7
  311.1 9.5 %all-to-all-start.4 = ((f32[64,1,512]{2,1,0:T(1,128)}), f32[64,1,512]{2,1,0:T(1,128)S(1)}, u32[]{:S(2)}, u32[]{:S(2)}) async-start(f32[64,1,512]{2,1,0:T(1,128)} %broadcast_in_dim.7), calls=%async_computation.4 | async-start | bytes 262144 | tf_op jit(solution)/shard_map/all_to_all | solution.py:12
  320.5 0.1 convert_element_type.15
  320.6 0.0 copy-done.4
  320.6 0.1 dynamic_slice.15
  320.7 16.0 %all-to-all-done.4 = f32[64,1,512]{2,1,0:T(1,128)S(1)} async-done(((f32[64,1,512]{2,1,0:T(1,128)}), f32[64,1,512]{2,1,0:T(1,128)S(1)}, u32[]{:S(2)}, u32[]{:S(2)}) %all-to-all-start.4) | async-done | bytes 131104 | tf_op jit(solution)/shard_map/all_to_all | solution.py:12
  336.7 0.1 reduce_sum.49
  336.8 0.1 fusion.13
  336.9 12.3 %all_gather.11 = bf16[512,256]{0,1:T(8,128)(2,1)S(1)} all-gather(bf16[512,64]{0,1:T(8,128)(2,1)S(1)} %fusion.13), channel_id=1, replica_groups=mesh['ra'=16,'cb'=4,'dp'=8] {'cb'}, dimensions={1}, use_global_device_ids=true | all-gather | bytes 327680 | tf_op jit(solution)/shard_map/all_gather | solution.py:85
  349.2 0.8 copy.32
  (5 shorter events, 0.1 us)
Async XLA Ops:
  6.5 288.8 %copy-start = (bf16[2816,256]{1,0:T(8,128)(2,1)S(1)}, bf16[2816,256]{1,0:T(8,128)(2,1)}, u32[]{:S(2)}) copy-start(bf16[2816,256]{1,0:T(8,128)(2,1)} %param.14) | copy-start | bytes 4325380
  9.9 27.8 %all-to-all-start.1 = ((f32[16,1,512]{2,1,0:T(1,128)}), f32[16,1,512]{2,1,0:T(1,128)S(1)}, u32[]{:S(2)}, u32[]{:S(2)}) async-start(f32[16,1,512]{2,1,0:T(1,128)} %broadcast_in_dim.6), calls=%async_computation.1 | async-start | bytes 65536 | tf_op jit(solution)/shard_map/all_to_all | solution.py:12
  37.6 79.1 %all-to-all-start.2 = ((bf16[256,16,176]{0,2,1:T(8,128)(2,1)}), bf16[256,16,176]{0,2,1:T(8,128)(2,1)S(1)}, u32[]{:S(2)}, u32[]{:S(2)}) async-start(bf16[256,16,176]{0,2,1:T(8,128)(2,1)} %bitcast.41), calls=%async_computation.2 | async-start | bytes 2883584 | tf_op jit(solution)/shard_map/all_to_all | solution.py:54
  41.3 175.2 %all-gather.3.cloned.1.call-start = ((), (), s32[]{:S(2)}) async-start(), calls=%async_computation.5 | async-start | bytes 4456448 | tf_op jit(solution)/shard_map/all_gather | solution.py:57
  116.7 91.4 %all-to-all-start = ((bf16[256,16,176]{0,2,1:T(8,128)(2,1)}), bf16[256,16,176]{0,2,1:T(8,128)(2,1)}, u32[]{:S(2)}, u32[]{:S(2)}) async-start(bf16[256,16,176]{0,2,1:T(8,128)(2,1)} %bitcast.40), calls=%async_computation | async-start | bytes 2883584 | tf_op jit(solution)/shard_map/all_to_all | solution.py:53
  127.0 168.4 %all-gather.5.cloned.1.call-start = ((), (), s32[]{:S(2)}) async-start(), calls=%async_computation.6 | async-start | bytes 3063808 | tf_op jit(solution)/shard_map/all_gather | solution.py:70
  208.2 8.4 %copy-start.2 = (bf16[16,22,8,256]{3,2,0,1:T(8,128)(2,1)S(1)}, bf16[16,22,8,256]{3,2,0,1:T(8,128)(2,1)}, u32[]{:S(2)}) copy-start(bf16[16,22,8,256]{3,2,0,1:T(8,128)(2,1)} %copy.36) | copy-start | bytes 4325380
  216.5 3.4 copy-start.1
  216.5 3.9 %copy-start.3 = (bf16[16,22,8,256]{3,2,0,1:T(8,128)(2,1)S(1)}, bf16[16,22,8,256]{3,2,0,1:T(8,128)(2,1)}, u32[]{:S(2)}) copy-start(bf16[16,22,8,256]{3,2,0,1:T(8,128)(2,1)} %copy.35) | copy-start | bytes 4325380
  298.1 22.5 %copy-start.4 = (f32[256]{0:T(256)S(1)}, f32[256]{0:T(256)}, u32[]{:S(2)}) copy-start(f32[256]{0:T(256)} %param.15) | copy-start | bytes 3076
  311.1 25.6 %all-to-all-start.4 = ((f32[64,1,512]{2,1,0:T(1,128)}), f32[64,1,512]{2,1,0:T(1,128)S(1)}, u32[]{:S(2)}, u32[]{:S(2)}) async-start(f32[64,1,512]{2,1,0:T(1,128)} %broadcast_in_dim.7), calls=%async_computation.4 | async-start | bytes 262144 | tf_op jit(solution)/shard_map/all_to_all | solution.py:12
Sparse Core Ops, SparseCore 0:
  44.2 172.2 all-gather.2
  222.9 72.3 all-gather.4
where the time goes:
time: 357 us
  waiting for transfers between devices  256 us (72%)
  starting transfers between devices  38.7 us (11%)
  blocking collectives  24.4 us (7%)
  local copies, waits for them, and re-layouts  14.4 us (4%)
  between operations  13.5 us (4%)
  matrix products  6.93 us (2%)
    all_to_all x1, waiting for transfers between devices, local(): lax.all_to_all(w_gate, 'ra', split_axis=1, concat_axis=0, tiled=True)  78.8 us
    all_gather x1, waiting for transfers between devices, local(): lax.all_gather(hidden, 'ra', axis=0, tiled=True)  72.5 us
    all_to_all x1, waiting for transfers between devices, local(): lax.all_to_all(w_up, 'ra', split_axis=1, concat_axis=0, tiled=True)  72.1 us
    all_to_all x2, waiting for transfers between devices, from_everyone(): lax.all_to_all(jnp.broadcast_to(array[None], (count, *array.shape)), axis...  26 us
    all_to_all x2, starting transfers between devices, from_everyone(): lax.all_to_all(jnp.broadcast_to(array[None], (count, *array.shape)), axis...  24.7 us
    all_gather x1, blocking collectives, local(): mixed = lax.all_gather(mixed_part, 'cb', axis=1, tiled=True)  12.3 us
    all_to_all x1, blocking collectives, summed_on_arrival(): tiles = lax.all_to_all(split_up(array, dim, count), axis, 0, 0, tiled=True)  12.1 us
    all_to_all x1, starting transfers between devices, local(): lax.all_to_all(w_gate, 'ra', split_axis=1, concat_axis=0, tiled=True)  10.3 us
  transfers between devices with their start and end apart: 6, of which 6 were waited for; matrix products, arithmetic and copies ran while one was open for 3% of the time, Pallas kernels for 0%

commit v1 on v0

v1 whole, which is shorter than its diff:
```python
import functools
import jax
import jax.numpy as jnp
from jax import lax
from jax.experimental import pallas as pl
from jax.experimental.pallas import tpu as pltpu
from jax.sharding import PartitionSpec as P

EPS = 1e-06
RESIDUAL = 0.125
MESH = pl.DeviceIdType.MESH
BF16 = jnp.bfloat16
F32 = jnp.float32


def _kernel(
    dim_full,
    nz,
    xw_ref, sq_ref, ws_ref, taps_ref, wd_ref, tok_ref, gain_ref,
    out_ref,
    xfull, wfull, hfull, acc, part, psend, precv, sq_all, psq_own, psq_all, mshare,
    xz_s, xz_r, y1_s, y1_r, y2_s, y2_r, wz_s, wz_r, wx_s, wx_r, wo_s, wo_r, wp_s, wp_r,
    sq_s, sq_r, hz_s, hz_r, ps_s, ps_r, pq_s, pq_r, mo_s, mo_r,
):
    half = nz // 2
    z = lax.axis_index("ra")
    y = lax.axis_index("cb")
    dp = lax.axis_index("dp")
    tokens, kb = xw_ref.shape
    quarter = tokens // 4
    qhalf = quarter // 2
    units = hfull.shape[2]
    hcols = hfull.shape[3]

    def zmod(v):
        return lax.rem(v + 2 * nz, nz)

    z_right, z_left = zmod(z + 1), zmod(z - 1)
    y_right, y_left, y_far = lax.rem(y + 1, 4), lax.rem(y + 3, 4), lax.rem(y + 2, 4)
    x_right, x_left = lax.rem(dp + 2, 8), lax.rem(dp + 6, 8)
    x_far = lax.rem(dp + 4, 8)
    partner = dp + 1 - 2 * lax.rem(dp, 2)

    def other(v):
        return v + 1 - 2 * lax.rem(v, 2)

    def rcopy(src, dst, ssem, rsem, dev):
        return pltpu.make_async_remote_copy(
            src_ref=src, dst_ref=dst, send_sem=ssem, recv_sem=rsem,
            device_id=dev, device_id_type=MESH,
        )

    bar = pltpu.get_barrier_semaphore()

    @pl.loop(1, nz)
    def _(d):
        pl.semaphore_signal(bar, inc=1, device_id={"ra": zmod(z + d)}, device_id_type=MESH)

    for t in (y_right, y_left, y_far):
        pl.semaphore_signal(bar, inc=1, device_id={"cb": t}, device_id_type=MESH)
    for t in (x_right, x_left, partner):
        pl.semaphore_signal(bar, inc=1, device_id={"dp": t}, device_id_type=MESH)
    pl.semaphore_wait(bar, nz - 1 + 6)

    def q_rows(q):
        return pl.ds(pl.multiple_of(q * quarter, quarter), quarter)

    def qh_rows(q, i):
        return pl.ds(pl.multiple_of(q * quarter + i * qhalf, qhalf), qhalf)

    def xz_copy(b, right, src=None):
        dst = xfull.at[b, q_rows(y)]
        return rcopy(dst if src is None else src, dst, xz_s.at[1 - right, b], xz_r.at[b],
                     {"ra": z_right if right else z_left})

    def y1_copy(b, right, q):
        ref = xfull.at[b, q_rows(q)]
        return rcopy(ref, ref, y1_s.at[1 - right, b], y1_r.at[1 - right, b],
                     {"cb": y_right if right else y_left})

    def y2_copy(b, right, q):
        ref = xfull.at[b, qh_rows(q, 1 - right)]
        return rcopy(ref, ref, y2_s.at[1 - right, b], y2_r.at[1 - right, b],
                     {"cb": y_right if right else y_left})

    def wz_copy(dest, source):
        return rcopy(ws_ref.at[dest], wfull.at[source, dp], wz_s.at[dest], wz_r.at[source],
                     {"ra": dest})

    def wx_copy(b, right, share, src=None):
        ref = wfull.at[b, share]
        return rcopy(ref if src is None else src, ref, wx_s.at[1 - right, b], wx_r.at[1 - right, b],
                     {"dp": x_right if right else x_left})

    def wo_copy(b, right, share):
        ref = wfull.at[b, share]
        return rcopy(ref, ref, wo_s.at[b], wo_r.at[b], {"dp": x_right if right else x_left})

    def wp_copy(b, k, share, src=None):
        ref = wfull.at[b, share]
        return rcopy(ref if src is None else src, ref, wp_s.at[k, b], wp_r.at[k, b], {"dp": partner})

    def sq_copy(dest, source):
        return rcopy(sq_ref, sq_all.at[source], sq_s.at[dest], sq_r.at[source], {"ra": dest})

    def w_issue(d):
        wz_copy(zmod(z + d), z).start()

        @pl.when(d < half)
        def _():
            wz_copy(zmod(z - d), z).start()

    def both(d, fn):
        fn(zmod(z - d))

        @pl.when((d > 0) & (d < half))
        def _():
            fn(zmod(z + d))

    def w_arrive(b):
        wz_copy(b, b).wait_recv()
        wp_copy(b, 0, dp).start()
        wx_copy(b, 1, dp).start()
        wx_copy(b, 0, dp).start()

    def w_side(b):
        wx_copy(b, 1, x_left).wait_recv()
        wx_copy(b, 0, x_right).wait_recv()
        wp_copy(b, 1, x_left).start()
        wp_copy(b, 2, x_right).start()

        @pl.when(lax.rem(b, 2) == 0)
        def _():
            wo_copy(b, 1, x_left).start()

        @pl.when(lax.rem(b, 2) == 1)
        def _():
            wo_copy(b, 0, x_right).start()

    def w_far(b):
        wo_copy(b, 1, x_far).wait_recv()
        wp_copy(b, 3, x_far).start()

    def w_last(b):
        wp_copy(b, 0, partner).wait_recv()
        wp_copy(b, 1, other(x_left)).wait_recv()
        wp_copy(b, 2, other(x_right)).wait_recv()
        wp_copy(b, 3, other(x_far)).wait_recv()

    def x_first(b):
        y1_copy(b, 1, y).start()
        y1_copy(b, 0, y).start()

    def x_second(b):
        y1_copy(b, 1, y_left).wait_recv()
        y2_copy(b, 1, y_left).start()
        y1_copy(b, 0, y_right).wait_recv()
        y2_copy(b, 0, y_right).start()

    def x_third(b):
        y2_copy(b, 1, y_far).wait_recv()
        y2_copy(b, 0, y_far).wait_recv()

    xz_copy(z, 1, xw_ref.at[q_rows(y)]).start()
    xz_copy(z, 0, xw_ref.at[q_rows(y)]).start()
    w_issue(1)
    w_issue(2)
    wp_copy(z, 0, dp, ws_ref.at[z]).start()
    wx_copy(z, 1, dp, ws_ref.at[z]).start()
    wx_copy(z, 0, dp, ws_ref.at[z]).start()

    @pl.loop(1, nz)
    def _(d):
        sq_copy(zmod(z + d), z).start()

    wfull[z, dp] = ws_ref[z]
    sq_all[z] = sq_ref[...]
    xfull[z] = xw_ref[...]

    groups = half // 2

    def group(g, fn):
        both(2 * g - 1, fn)
        both(2 * g, fn)

    @pl.loop(1, half + 3)
    def _(s):
        @pl.when(s <= half)
        def _():
            br = zmod(z - s)
            xz_copy(br, 1).wait_recv()

            @pl.when(s < half)
            def _():
                xz_copy(br, 1).start()

            x_first(br)

            @pl.when(s < half)
            def _():
                bl = zmod(z + s)
                xz_copy(bl, 0).wait_recv()

                @pl.when(s < half - 1)
                def _():
                    xz_copy(bl, 0).start()

                x_first(bl)

        @pl.when(s < groups)
        def _():
            w_issue(2 * s + 1)
            w_issue(2 * s + 2)

        @pl.when((s >= 2) & (s <= half + 1))
        def _():
            both(s - 1, x_second)

        @pl.when(s >= 3)
        def _():
            both(s - 2, x_third)

        @pl.when(s == 2)
        def _():
            w_side(z)

        @pl.when(s == 3)
        def _():
            w_far(z)

        @pl.when((s >= 2) & (s < groups + 2))
        def _():
            group(s - 1, w_arrive)

        @pl.when((s >= 3) & (s < groups + 3))
        def _():
            group(s - 2, w_side)

        @pl.when((s >= 4) & (s < groups + 4))
        def _():
            group(s - 3, w_far)

    @pl.loop(0, half + 1)
    def _(d):
        both(d, w_last)

    acc[...] = jnp.zeros_like(acc)

    @pl.loop(0, nz)
    def _(b):
        w = wfull[b].reshape(kb, acc.shape[1])
        acc[...] += jnp.dot(xfull[b], w, preferred_element_type=F32)

    @pl.loop(1, nz)
    def _(d):
        src = zmod(z + d)
        sq_copy(src, src).wait_recv()

    scale = lax.rsqrt(jnp.sum(sq_all[...], axis=0) / dim_full + EPS)
    lin = jnp.transpose(acc[...], (1, 0))

    def conv(field, base):
        lane = lax.broadcasted_iota(jnp.int32, field.shape, 1)
        before = jnp.where(lane == 0, 0.0, pltpu.roll(field, 1, 1))
        after = jnp.where(lane == tokens - 1, 0.0, pltpu.roll(field, tokens - 1, 1))
        return (
            taps_ref[:, base : base + 1] * before
            + taps_ref[:, base + 1 : base + 2] * field
            + taps_ref[:, base + 2 : base + 3] * after
        )

    gate = conv(lin[:units] * scale, 0)
    up = conv(lin[units : 2 * units] * scale, 3)
    hidden = (jax.nn.gelu(gate, approximate=True) * up).astype(BF16)
    subs = tokens // hcols
    for c in range(subs):
        hfull[z, c] = hidden[:, c * hcols : (c + 1) * hcols]

    def hz_copy(b, c, right):
        ref = hfull.at[b, c]
        return rcopy(ref, ref, hz_s.at[1 - right, b, c], hz_r.at[b, c],
                     {"ra": z_right if right else z_left})

    for c in range(subs):
        hz_copy(z, c, 1).start()
        hz_copy(z, c, 0).start()

    def down(b, c, first=False):
        w = wd_ref[pl.ds(pl.multiple_of(b * units, units), units), :]
        value = lax.dot_general(w, hfull[b, c], (((0,), (0,)), ((), ())), preferred_element_type=F32)
        cols = pl.ds(c * hcols, hcols)
        if first:
            part[:, cols] = value
        else:
            part[:, cols] += value

    for c in range(subs):
        down(z, c, True)

    @pl.loop(1, half)
    def _(s):
        br, bl = zmod(z - s), zmod(z + s)
        for c in range(subs):
            hz_copy(br, c, 1).wait_recv()
            if c < subs // 2:
                hz_copy(br, c, 1).start()
            else:
                @pl.when(s < half - 1)
                def _():
                    hz_copy(br, c, 1).start()
            hz_copy(bl, c, 0).wait_recv()
            if c >= subs // 2:
                hz_copy(bl, c, 0).start()
            else:
                @pl.when(s < half - 1)
                def _():
                    hz_copy(bl, c, 0).start()
        for c in range(subs):
            down(br, c)
            down(bl, c)

    far = zmod(z + half)
    for c in range(subs):
        hz_copy(far, c, 1 if c < subs // 2 else 0).wait_recv()
        down(far, c)

    def ps_copy(k, dest):
        return rcopy(psend.at[k], precv.at[k], ps_s.at[k], ps_r.at[k], {"cb": dest})

    def quarter_cols(q):
        return pl.ds(pl.multiple_of(q * quarter, quarter), quarter)

    for k, dest in enumerate((y_far, y_right, y_left)):
        psend[k] = part[:, quarter_cols(dest)].astype(BF16)
        ps_copy(k, dest).start()
    share = part[:, quarter_cols(y)]
    for k, dest in enumerate((y_far, y_right, y_left)):
        ps_copy(k, dest).wait_recv()
        share = share + precv[k].astype(F32)

    def pq_copy(dest, source):
        return rcopy(psq_own, psq_all.at[source], pq_s.at[dest], pq_r.at[source], {"ra": dest})

    own_sq = jnp.sum(share * share, axis=0, keepdims=True)
    psq_own[...] = own_sq
    psq_all[z] = own_sq

    @pl.loop(1, nz)
    def _(d):
        pq_copy(zmod(z + d), z).start()

    branch = jnp.transpose(share, (1, 0)) * gain_ref[...]
    base = RESIDUAL * tok_ref[q_rows(y), :].astype(F32)

    @pl.loop(1, nz)
    def _(d):
        src = zmod(z + d)
        pq_copy(src, src).wait_recv()

    post = lax.rsqrt(jnp.sum(psq_all[...], axis=0) / dim_full + EPS)
    post_col = jnp.transpose(jnp.broadcast_to(post, (quarter, quarter)), (1, 0))[:, :1]
    mixed = (base + branch * post_col).astype(BF16)
    mshare[...] = mixed
    out_ref[q_rows(y), :] = mixed

    def mo_copy(k, dest, q):
        return rcopy(mshare, out_ref.at[q_rows(q)], mo_s.at[k], mo_r.at[k], {"cb": dest})

    for k, dest in enumerate((y_far, y_right, y_left)):
        mo_copy(k, dest, y).start()
    for k, source in enumerate((y_far, y_left, y_right)):
        mo_copy(k, source, source).wait_recv()

    @pl.loop(0, half + 1)
    def _(s):
        @pl.when(s < half)
        def _():
            xz_copy(zmod(z - s), 1).wait_send()
            hz_copy(zmod(z - s), 0, 1).wait_send()

        @pl.when(s < half - 1)
        def _():
            xz_copy(zmod(z + s), 0).wait_send()

        for c in range(subs):
            first = c < subs // 2

            @pl.when(s < (half if first else half - 1))
            def _():
                if c > 0:
                    hz_copy(zmod(z - s), c, 1).wait_send()

            @pl.when(s < (half - 1 if first else half))
            def _():
                hz_copy(zmod(z + s), c, 0).wait_send()

    @pl.loop(0, nz)
    def _(b):
        @pl.when(b != z)
        def _():
            y1_copy(b, 1, y).wait_send()
            y1_copy(b, 0, y).wait_send()
            y2_copy(b, 1, y_left).wait_send()
            y2_copy(b, 0, y_right).wait_send()
            wz_copy(b, z).wait_send()
            sq_copy(b, z).wait_send()
            pq_copy(b, z).wait_send()

        wx_copy(b, 1, dp).wait_send()
        wx_copy(b, 0, dp).wait_send()
        wo_copy(b, 1, x_left).wait_send()
        for k in range(4):
            wp_copy(b, k, dp).wait_send()

    for k, dest in enumerate((y_far, y_right, y_left)):
        ps_copy(k, dest).wait_send()
        mo_copy(k, dest, y).wait_send()


def local(tokens, pre_gain, w_gate, w_up, conv_gate, conv_up, w_down, post_gain):
    nz = lax.axis_size("ra")
    _, positions, kb = tokens.shape
    ff = w_gate.shape[1]
    units = ff // nz
    lanes = -(-2 * units // 128) * 128
    rows = kb // 8
    quarter = positions // 4
    subs = 2
    dim_full = kb * nz
    tok = tokens[0]
    values = tok.astype(F32)
    sq = jnp.sum(values * values, axis=1)[None, :]
    weighted = (values * pre_gain).astype(BF16)
    row = lax.axis_index("dp") * rows

    def pieces(w):
        own = lax.dynamic_slice_in_dim(w, row, rows, 0)
        return own.reshape(rows, nz, units).transpose(1, 0, 2)

    ws = jnp.concatenate(
        [pieces(w_gate), pieces(w_up), jnp.zeros((nz, rows, lanes - 2 * units), BF16)], axis=2
    )
    start = lax.axis_index("ra") * units
    taps = jnp.concatenate(
        [
            lax.dynamic_slice_in_dim(conv_gate, start, units, 1),
            lax.dynamic_slice_in_dim(conv_up, start, units, 1),
        ],
        axis=0,
    ).T

    dma = pltpu.SemaphoreType.DMA
    vmem = pltpu.VMEM
    scratch = [
        vmem((nz, positions, kb), BF16),
        vmem((nz, 8, rows, lanes), BF16),
        vmem((nz, subs, units, positions // subs), BF16),
        vmem((positions, lanes), F32),
        vmem((kb, positions), F32),
        vmem((3, kb, quarter), BF16),
        vmem((3, kb, quarter), BF16),
        vmem((nz, 1, positions), F32),
        vmem((1, quarter), F32),
        vmem((nz, 1, quarter), F32),
        vmem((quarter, kb), BF16),
        dma((2, nz)), dma((nz,)),
        dma((2, nz)), dma((2, nz)), dma((2, nz)), dma((2, nz)),
        dma((nz,)), dma((nz,)), dma((2, nz)), dma((2, nz)), dma((nz,)), dma((nz,)),
        dma((4, nz)), dma((4, nz)),
        dma((nz,)), dma((nz,)), dma((2, nz, subs)), dma((nz, subs)),
        dma((3,)), dma((3,)), dma((nz,)), dma((nz,)), dma((3,)), dma((3,)),
    ]

    out = pl.pallas_call(
        functools.partial(_kernel, dim_full, nz),
        out_shape=jax.ShapeDtypeStruct((positions, kb), BF16),
        in_specs=[pl.BlockSpec(memory_space=pltpu.VMEM)] * 7,
        out_specs=pl.BlockSpec(memory_space=pltpu.VMEM),
        scratch_shapes=scratch,
        name="ffn",
        compiler_params=pltpu.CompilerParams(
            collective_id=0, has_side_effects=True, vmem_limit_bytes=48 * 1024 * 1024
        ),
    )(weighted, sq, ws, taps, w_down, tok, post_gain[None, :])
    return out[None]


def solution(mesh):
    in_specs = (
        P("dp", None, "ra"),
        P("ra"),
        P("ra", "cb"),
        P("ra", "cb"),
        P(None, "cb"),
        P(None, "cb"),
        P("cb", "ra"),
        P("ra"),
    )
    out_specs = P("dp", None, "ra")
    return jax.shard_map(local, mesh=mesh, in_specs=in_specs, out_specs=out_specs, check_vma=False)
```

time: 357 us -> 133 us (0.37)
  waiting for transfers between devices: 256 us -> 0 us
  Pallas kernels: 0 us -> 129 us
  starting transfers between devices: 38.7 us -> 0 us
  blocking collectives: 24.4 us -> 0 us
  between operations: 13.5 us -> 0.13 us
  local copies, waits for them, and re-layouts: 14.4 us -> 3.87 us
  matrix products: 6.93 us -> 0 us
    all_to_all x4 -> x0, waiting for transfers between devices: 177 us -> none  [the longest x1 78.8 us: local(): lax.all_to_all(w_gate, 'ra', split_axis=1, concat_axis=0, tiled=True)]
    pallas_call x0 -> x1, Pallas kernels: none -> 129 us  [local(): pl.pallas_call(functools.partial(_kernel, dim_full, nz), out_shape=jax.Sh...]
    all_gather x2 -> x0, waiting for transfers between devices: 78.1 us -> none  [the longest x1 72.5 us: local(): lax.all_gather(hidden, 'ra', axis=0, tiled=True)]
    all_to_all x4 -> x0, starting transfers between devices: 38.6 us -> none  [the longest x2 24.7 us: from_everyone(): lax.all_to_all(jnp.broadcast_to(array[None], (count, *array.shape)), axis...]
    all_gather x1 -> x0, blocking collectives: 12.3 us -> none  [local(): mixed = lax.all_gather(mixed_part, 'cb', axis=1, tiled=True)]
    all_to_all x1 -> x0, blocking collectives: 12.1 us -> none  [summed_on_arrival(): tiles = lax.all_to_all(split_up(array, dim, count), axis, 0, 0, tiled=True)]
    dot_general x3 -> x0, matrix products: 6.93 us -> none  [the longest x1 3.25 us: local(): lax.dot_general(up_cols, piece, dims, preferred_element_type=jnp.float32)]
    unnamed x13 -> x9, local copies, waits for them, and re-layouts: 6.94 us -> 0.73 us
  transfers between devices with their start and end apart: 6 -> 0, of which waited for: 6 -> 0; matrix products, arithmetic and copies ran while one was open for 3% -> 0% of each run, Pallas kernels for 0% -> 0%
where the time goes in v1:
time: 133 us
  Pallas kernels  129 us (97%)
  local copies, waits for them, and re-layouts  3.87 us (3%)
    pallas_call x1, Pallas kernels, local(): pl.pallas_call(functools.partial(_kernel, dim_full, nz), out_shape=jax.Sh...  129 us

profile of v1, /device:TPU:6, one launch (start us, length us, event | category | flops | bytes accessed | tf_op | source)
XLA Modules:
  0.0 133.3 jit_solution(6573655666346268746)
XLA Ops:
  0.0 1.0 constant_dynamic-slice_fusion.2
  1.0 0.0 copy-start.1
  1.0 0.0 copy-start.3
  1.1 0.5 reshape.8
  1.5 0.0 copy-start
  1.6 0.0 copy-start.2
  1.6 0.1 copy.20
  1.7 0.5 reshape.7
  2.1 0.1 copy.21
  2.2 0.1 pad.4.clone
  2.3 0.2 maximum_maximum_fusion.ws_ref
  2.5 0.8 constant_dynamic-slice_fusion
  3.3 0.1 copy.17
  3.4 0.0 copy-done.1
  3.4 0.0 copy-done.3
  3.4 0.2 fusion.1
  3.6 0.0 copy-done
  3.6 0.0 copy-done.2
  3.6 128.9 %ffn.1 = bf16[512,256]{1,0:T(8,128)(2,1)S(1)} custom-call(bf16[512,256]{1,0:T(8,128)(2,1)S(1)} %get-tuple-element.6.xw_ref, f32[1,512]{1,0:T(1,128)S(1)} %bitcast.16, bf16[16,32,384]{2,1,0:T(8,128)(2,1)S(1)} %maximum_maximum_fusion.ws_ref, f32[176,6]{1,0:T(8,128)S(1)} %bitcast.15, bf16[2816,256]{1,0:T(8,128)(2,1)S(1)} %copy-done, ...), custom_call_target="tpu_custom_call" | custom-call | tf_op jit(solution)/shard_map/ffn/pallas_call | solution.py:474
  132.5 0.7 copy.23
  (2 shorter events, 0.0 us)
Async XLA Ops:
  1.0 2.4 %copy-start.1 = (bf16[1,512,256]{2,1,0:T(8,128)(2,1)S(1)}, bf16[1,512,256]{2,1,0:T(8,128)(2,1)}, u32[]{:S(2)}) copy-start(bf16[1,512,256]{2,1,0:T(8,128)(2,1)} %param.8) | copy-start | bytes 786436
  1.0 2.4 %copy-start.3 = (f32[256]{0:T(256)S(1)}, f32[256]{0:T(256)}, u32[]{:S(2)}) copy-start(f32[256]{0:T(256)} %param.9) | copy-start | bytes 3076
  1.5 2.0 %copy-start = (bf16[2816,256]{1,0:T(8,128)(2,1)S(1)}, bf16[2816,256]{1,0:T(8,128)(2,1)}, u32[]{:S(2)}) copy-start(bf16[2816,256]{1,0:T(8,128)(2,1)} %wd_ref.1) | copy-start | bytes 4325380
  1.6 2.0 %copy-start.2 = (f32[256]{0:T(256)S(1)}, f32[256]{0:T(256)}, u32[]{:S(2)}) copy-start(f32[256]{0:T(256)} %param.15) | copy-start | bytes 3076

commit v2 on v1

--- a/solution.py
+++ b/solution.py
@@ -16,11 +16,13 @@
 def _kernel(
     dim_full,
     nz,
-    xw_ref, sq_ref, ws_ref, taps_ref, wd_ref, tok_ref, gain_ref,
+    tok_ref, pre_ref, wg_ref, wu_ref, cg_ref, cu_ref, wd_hbm, gain_ref,
     out_ref,
-    xfull, wfull, hfull, acc, part, psend, precv, sq_all, psq_own, psq_all, mshare,
+    xw_ref, sq_ref, ws_ref, wrows, wd_ref, taps_in, taps_ref,
+    xfull, wfull, hfull, acc, part, psend, precv, sq_all, psq_own, psq_all,
+    bshare, bfull, post_own, post_all, in_sem,
     xz_s, xz_r, y1_s, y1_r, y2_s, y2_r, wz_s, wz_r, wx_s, wx_r, wo_s, wo_r, wp_s, wp_r,
-    sq_s, sq_r, hz_s, hz_r, ps_s, ps_r, pq_s, pq_r, mo_s, mo_r,
+    sq_s, sq_r, hz_s, hz_r, ps_s, ps_r, pq_s, pq_r, mo_s, mo_r, po_s, po_r,
 ):
     half = nz // 2
     z = lax.axis_index("ra")
@@ -29,8 +31,9 @@
     tokens, kb = xw_ref.shape
     quarter = tokens // 4
     qhalf = quarter // 2
-    units = hfull.shape[2]
-    hcols = hfull.shape[3]
+    units = hfull.shape[1]
+    rows = wrows.shape[1]
+    lanes = acc.shape[1]
 
     def zmod(v):
         return lax.rem(v + 2 * nz, nz)
@@ -60,6 +63,27 @@
         pl.semaphore_signal(bar, inc=1, device_id={"cb": t}, device_id_type=MESH)
     for t in (x_right, x_left, partner):
         pl.semaphore_signal(bar, inc=1, device_id={"dp": t}, device_id_type=MESH)
+
+    own = pl.ds(pl.multiple_of(dp * rows, rows), rows)
+    loads = [
+        pltpu.make_async_copy(wg_ref.at[own], wrows.at[0], in_sem.at[0]),
+        pltpu.make_async_copy(wu_ref.at[own], wrows.at[1], in_sem.at[1]),
+        pltpu.make_async_copy(wd_hbm, wd_ref, in_sem.at[2]),
+    ]
+    for load in loads:
+        load.start()
+    values = tok_ref[...].astype(F32)
+    xw_ref[...] = (values * pre_ref[...]).astype(BF16)
+    sq_ref[...] = jnp.sum(jnp.transpose(values * values, (1, 0)), axis=0, keepdims=True)
+    loads[0].wait()
+    loads[1].wait()
+    tail = jnp.zeros((rows, lanes - 2 * units), BF16)
+    for j in range(nz):
+        cut = slice(j * units, (j + 1) * units)
+        ws_ref[j] = jnp.concatenate([wrows[0, :, cut], wrows[1, :, cut], tail], axis=1)
+    xfull[z] = xw_ref[...]
+    wfull[z, dp] = ws_ref[z]
+    sq_all[z] = sq_ref[...]
     pl.semaphore_wait(bar, nz - 1 + 6)
 
     def q_rows(q):
@@ -173,17 +197,27 @@
     def _(d):
         sq_copy(zmod(z + d), z).start()
 
-    wfull[z, dp] = ws_ref[z]
-    sq_all[z] = sq_ref[...]
-    xfull[z] = xw_ref[...]
-
-    groups = half // 2
-
-    def group(g, fn):
-        both(2 * g - 1, fn)
-        both(2 * g, fn)
-
-    @pl.loop(1, half + 3)
+    acc[...] = jnp.zeros_like(acc)
+    taps_in[0:3] = cg_ref[...]
+    taps_in[3:6] = cu_ref[...]
+    taps_in[6:8] = jnp.zeros((2, taps_in.shape[1]), F32)
+    taps_ref[...] = jnp.transpose(taps_in[...], (1, 0))
+
+    def product(b):
+        w_last(b)
+        w = wfull[b].reshape(kb, lanes)
+        acc[...] += jnp.dot(xfull[b], w, preferred_element_type=F32)
+
+    def with_first(d, fn):
+        @pl.when((d >= 2) & (d <= half))
+        def _():
+            @pl.when(d == 2)
+            def _():
+                both(1, fn)
+
+            both(d, fn)
+
+    @pl.loop(1, half + 4)
     def _(s):
         @pl.when(s <= half)
         def _():
@@ -207,49 +241,37 @@
 
                 x_first(bl)
 
-        @pl.when(s < groups)
-        def _():
-            w_issue(2 * s + 1)
-            w_issue(2 * s + 2)
+        @pl.when(s + 2 <= half)
+        def _():
+            w_issue(s + 2)
 
         @pl.when((s >= 2) & (s <= half + 1))
         def _():
             both(s - 1, x_second)
 
-        @pl.when(s >= 3)
+        with_first(s, w_arrive)
+
+        @pl.when(s == 1)
+        def _():
+            w_side(z)
+
+        with_first(s - 1, w_side)
+
+        @pl.when(s == 2)
+        def _():
+            w_far(z)
+
+        with_first(s - 2, w_far)
+
+        @pl.when((s >= 3) & (s <= half + 2))
         def _():
             both(s - 2, x_third)
 
-        @pl.when(s == 2)
-        def _():
-            w_side(z)
-
         @pl.when(s == 3)
         def _():
-            w_far(z)
-
-        @pl.when((s >= 2) & (s < groups + 2))
-        def _():
-            group(s - 1, w_arrive)
-
-        @pl.when((s >= 3) & (s < groups + 3))
-        def _():
-            group(s - 2, w_side)
-
-        @pl.when((s >= 4) & (s < groups + 4))
-        def _():
-            group(s - 3, w_far)
-
-    @pl.loop(0, half + 1)
-    def _(d):
-        both(d, w_last)
-
-    acc[...] = jnp.zeros_like(acc)
-
-    @pl.loop(0, nz)
-    def _(b):
-        w = wfull[b].reshape(kb, acc.shape[1])
-        acc[...] += jnp.dot(xfull[b], w, preferred_element_type=F32)
+            product(z)
+
+        with_first(s - 3, product)
 
     @pl.loop(1, nz)
     def _(d):
@@ -258,26 +280,28 @@
 
     scale = lax.rsqrt(jnp.sum(sq_all[...], axis=0) / dim_full + EPS)
     lin = jnp.transpose(acc[...], (1, 0))
+    taps = taps_ref[pl.ds(pl.multiple_of(z * units, units), units), :]
 
     def conv(field, base):
         lane = lax.broadcasted_iota(jnp.int32, field.shape, 1)
         before = jnp.where(lane == 0, 0.0, pltpu.roll(field, 1, 1))
         after = jnp.where(lane == tokens - 1, 0.0, pltpu.roll(field, tokens - 1, 1))
         return (
-            taps_ref[:, base : base + 1] * before
-            + taps_ref[:, base + 1 : base + 2] * field
-            + taps_ref[:, base + 2 : base + 3] * after
+            taps[:, base : base + 1] * before
+            + taps[:, base + 1 : base + 2] * field
+            + taps[:, base + 2 : base + 3] * after
         )
 
     gate = conv(lin[:units] * scale, 0)
     up = conv(lin[units : 2 * units] * scale, 3)
     hidden = (jax.nn.gelu(gate, approximate=True) * up).astype(BF16)
-    subs = tokens // hcols
-    for c in range(subs):
-        hfull[z, c] = hidden[:, c * hcols : (c + 1) * hcols]
+    hfull[z] = hidden
+    step_rows = -(-units // 64) * 16
+    cuts = [(r, min(step_rows, units - r)) for r in range(0, units, step_rows)]
+    subs = len(cuts)
 
     def hz_copy(b, c, right):
-        ref = hfull.at[b, c]
+        ref = hfull.at[b, pl.ds(*cuts[c])]
         return rcopy(ref, ref, hz_s.at[1 - right, b, c], hz_r.at[b, c],
                      {"ra": z_right if right else z_left})
 
@@ -285,17 +309,12 @@
         hz_copy(z, c, 1).start()
         hz_copy(z, c, 0).start()
 
-    def down(b, c, first=False):
+    def down(b):
         w = wd_ref[pl.ds(pl.multiple_of(b * units, units), units), :]
-        value = lax.dot_general(w, hfull[b, c], (((0,), (0,)), ((), ())), preferred_element_type=F32)
-        cols = pl.ds(c * hcols, hcols)
-        if first:
-            part[:, cols] = value
-        else:
-            part[:, cols] += value
-
-    for c in range(subs):
-        down(z, c, True)
+        return lax.dot_general(w, hfull[b], (((0,), (0,)), ((), ())), preferred_element_type=F32)
+
+    loads[2].wait()
+    part[...] = down(z)
 
     @pl.loop(1, half)
     def _(s):
@@ -315,14 +334,13 @@
                 @pl.when(s < half - 1)
                 def _():
                     hz_copy(bl, c, 0).start()
-        for c in range(subs):
-            down(br, c)
-            down(bl, c)
+        part[...] += down(br)
+        part[...] += down(bl)
 
     far = zmod(z + half)
     for c in range(subs):
         hz_copy(far, c, 1 if c < subs // 2 else 0).wait_recv()
-        down(far, c)
+    part[...] += down(far)
 
     def ps_copy(k, dest):
         return rcopy(psend.at[k], precv.at[k], ps_s.at[k], ps_r.at[k], {"cb": dest})
@@ -350,7 +368,17 @@
         pq_copy(zmod(z + d), z).start()
 
     branch = jnp.transpose(share, (1, 0)) * gain_ref[...]
-    base = RESIDUAL * tok_ref[q_rows(y), :].astype(F32)
+    bshare[...] = branch.astype(BF16)
+
+    def mo_copy(k, dest):
+        return rcopy(bshare, bfull.at[k], mo_s.at[k], mo_r.at[k], {"cb": dest})
+
+    def po_copy(k, dest):
+        return rcopy(post_own, post_all.at[k], po_s.at[k], po_r.at[k], {"cb": dest})
+
+    peers = (y_far, y_right, y_left)
+    for k, dest in enumerate(peers):
+        mo_copy(k, dest).start()
 
     @pl.loop(1, nz)
     def _(d):
@@ -358,41 +386,41 @@
         pq_copy(src, src).wait_recv()
 
     post = lax.rsqrt(jnp.sum(psq_all[...], axis=0) / dim_full + EPS)
-    post_col = jnp.transpose(jnp.broadcast_to(post, (quarter, quarter)), (1, 0))[:, :1]
-    mixed = (base + branch * post_col).astype(BF16)
-    mshare[...] = mixed
-    out_ref[q_rows(y), :] = mixed
-
-    def mo_copy(k, dest, q):
-        return rcopy(mshare, out_ref.at[q_rows(q)], mo_s.at[k], mo_r.at[k], {"cb": dest})
-
-    for k, dest in enumerate((y_far, y_right, y_left)):
-        mo_copy(k, dest, y).start()
+    post_own[...] = post
+    for k, dest in enumerate(peers):
+        po_copy(k, dest).start()
+
+    def finish(q, value, scale_row):
+        col = jnp.transpose(jnp.broadcast_to(scale_row, (quarter, quarter)), (1, 0))[:, :1]
+        base = RESIDUAL * tok_ref[q_rows(q), :].astype(F32)
+        out_ref[q_rows(q), :] = (base + value * col).astype(BF16)
+
+    finish(y, branch, post)
     for k, source in enumerate((y_far, y_left, y_right)):
-        mo_copy(k, source, source).wait_recv()
-
-    @pl.loop(0, half + 1)
-    def _(s):
-        @pl.when(s < half)
-        def _():
-            xz_copy(zmod(z - s), 1).wait_send()
-            hz_copy(zmod(z - s), 0, 1).wait_send()
-
-        @pl.when(s < half - 1)
-        def _():
-            xz_copy(zmod(z + s), 0).wait_send()
-
-        for c in range(subs):
-            first = c < subs // 2
-
-            @pl.when(s < (half if first else half - 1))
+        mo_copy(k, source).wait_recv()
+        po_copy(k, source).wait_recv()
+        finish(source, bfull[k].astype(F32), post_all[k])
+
+    for c in range(subs):
+        first = c < subs // 2
+
+        @pl.loop(0, half)
+        def _(t):
+            @pl.when(t < (half if first else half - 1))
             def _():
-                if c > 0:
-                    hz_copy(zmod(z - s), c, 1).wait_send()
-
-            @pl.when(s < (half - 1 if first else half))
+                hz_copy(zmod(z - t), c, 1).wait_send()
+
+            @pl.when(t < (half - 1 if first else half))
             def _():
-                hz_copy(zmod(z + s), c, 0).wait_send()
+                hz_copy(zmod(z + t), c, 0).wait_send()
+
+    @pl.loop(0, half)
+    def _(t):
+        xz_copy(zmod(z - t), 1).wait_send()
+
+        @pl.when(t < half - 1)
+        def _():
+            xz_copy(zmod(z + t), 0).wait_send()
 
     @pl.loop(0, nz)
     def _(b):
@@ -412,9 +440,10 @@
         for k in range(4):
             wp_copy(b, k, dp).wait_send()
 
-    for k, dest in enumerate((y_far, y_right, y_left)):
+    for k, dest in enumerate(peers):
         ps_copy(k, dest).wait_send()
-        mo_copy(k, dest, y).wait_send()
+        mo_copy(k, dest).wait_send()
+        po_copy(k, dest).wait_send()
 
 
 def local(tokens, pre_gain, w_gate, w_up, conv_gate, conv_up, w_down, post_gain):
@@ -425,36 +454,22 @@
     lanes = -(-2 * units // 128) * 128
     rows = kb // 8
     quarter = positions // 4
-    subs = 2
+    subs = -(-units // (-(-units // 64) * 16))
     dim_full = kb * nz
-    tok = tokens[0]
-    values = tok.astype(F32)
-    sq = jnp.sum(values * values, axis=1)[None, :]
-    weighted = (values * pre_gain).astype(BF16)
-    row = lax.axis_index("dp") * rows
-
-    def pieces(w):
-        own = lax.dynamic_slice_in_dim(w, row, rows, 0)
-        return own.reshape(rows, nz, units).transpose(1, 0, 2)
-
-    ws = jnp.concatenate(
-        [pieces(w_gate), pieces(w_up), jnp.zeros((nz, rows, lanes - 2 * units), BF16)], axis=2
-    )
-    start = lax.axis_index("ra") * units
-    taps = jnp.concatenate(
-        [
-            lax.dynamic_slice_in_dim(conv_gate, start, units, 1),
-            lax.dynamic_slice_in_dim(conv_up, start, units, 1),
-        ],
-        axis=0,
-    ).T
 
     dma = pltpu.SemaphoreType.DMA
     vmem = pltpu.VMEM
     scratch = [
+        vmem((positions, kb), BF16),
+        vmem((1, positions), F32),
+        vmem((nz, rows, lanes), BF16),
+        vmem((2, rows, ff), BF16),
+        vmem((ff, kb), BF16),
+        vmem((8, ff), F32),
+        vmem((ff, 8), F32),
         vmem((nz, positions, kb), BF16),
         vmem((nz, 8, rows, lanes), BF16),
-        vmem((nz, subs, units, positions // subs), BF16),
+        vmem((nz, units, positions), BF16),
         vmem((positions, lanes), F32),
         vmem((kb, positions), F32),
         vmem((3, kb, quarter), BF16),
@@ -463,25 +478,31 @@
         vmem((1, quarter), F32),
         vmem((nz, 1, quarter), F32),
         vmem((quarter, kb), BF16),
+        vmem((3, quarter, kb), BF16),
+        vmem((1, quarter), F32),
+        vmem((3, 1, quarter), F32),
+        dma((3,)),
         dma((2, nz)), dma((nz,)),
         dma((2, nz)), dma((2, nz)), dma((2, nz)), dma((2, nz)),
         dma((nz,)), dma((nz,)), dma((2, nz)), dma((2, nz)), dma((nz,)), dma((nz,)),
         dma((4, nz)), dma((4, nz)),
         dma((nz,)), dma((nz,)), dma((2, nz, subs)), dma((nz, subs)),
-        dma((3,)), dma((3,)), dma((nz,)), dma((nz,)), dma((3,)), dma((3,)),
+        dma((3,)), dma((3,)), dma((nz,)), dma((nz,)), dma((3,)), dma((3,)), dma((3,)), dma((3,)),
     ]
 
+    here = pl.BlockSpec(memory_space=pltpu.VMEM)
+    away = pl.BlockSpec(memory_space=pl.ANY)
     out = pl.pallas_call(
         functools.partial(_kernel, dim_full, nz),
         out_shape=jax.ShapeDtypeStruct((positions, kb), BF16),
-        in_specs=[pl.BlockSpec(memory_space=pltpu.VMEM)] * 7,
+        in_specs=[here, here, away, away, here, here, away, here],
         out_specs=pl.BlockSpec(memory_space=pltpu.VMEM),
         scratch_shapes=scratch,
         name="ffn",
         compiler_params=pltpu.CompilerParams(
             collective_id=0, has_side_effects=True, vmem_limit_bytes=48 * 1024 * 1024
         ),
-    )(weighted, sq, ws, taps, w_down, tok, post_gain[None, :])
+    )(tokens[0], pre_gain[None, :], w_gate, w_up, conv_gate, conv_up, w_down, post_gain[None, :])
     return out[None]
 
 

time: 133 us -> 129 us (0.970); the launches traced: 133 us -> 127 us
  Pallas kernels: 129 us -> 119 us
  local copies, waits for them, and re-layouts: 3.87 us -> 8.67 us
    pallas_call x1, Pallas kernels: 129 us -> 119 us  [local(): pl.pallas_call(functools.partial(_kernel, dim_full, nz), out_shape=jax.Sh...]
    unnamed x9 -> x17, local copies, waits for them, and re-layouts: 0.73 us -> 8.67 us
    dynamic_slice x2 -> x0, local copies, waits for them, and re-layouts: 1.82 us -> none  [the longest x1 1.03 us: pieces(): own = lax.dynamic_slice_in_dim(w, row, rows, 0)]
where the time goes in v2:
time: 129 us; the launch traced here: 127 us
  Pallas kernels  119 us (92%)
  local copies, waits for them, and re-layouts  8.67 us (7%)
    pallas_call x1, Pallas kernels, local(): pl.pallas_call(functools.partial(_kernel, dim_full, nz), out_shape=jax.Sh...  119 us
    unnamed x17, local copies, waits for them, and re-layouts  8.67 us

profile of v2, /device:TPU:6, one launch (start us, length us, event | category | flops | bytes accessed | tf_op | source)
XLA Modules:
  0.0 127.4 jit_solution(17697279223131075809)
XLA Ops:
  0.0 0.0 copy-start
  0.0 1.4 %copy-done = bf16[256,2816]{1,0:T(8,128)(2,1)S(1)} copy-done((bf16[256,2816]{1,0:T(8,128)(2,1)S(1)}, bf16[256,2816]{1,0:T(8,128)(2,1)}, u32[]{:S(2)}) %copy-start) | copy-done | bytes 1441816
  1.4 0.0 copy-start.1
  1.4 1.4 %copy-done.1 = bf16[256,2816]{1,0:T(8,128)(2,1)S(1)} copy-done((bf16[256,2816]{1,0:T(8,128)(2,1)S(1)}, bf16[256,2816]{1,0:T(8,128)(2,1)}, u32[]{:S(2)}) %copy-start.1) | copy-done | bytes 1441816
  2.7 0.0 copy-start.2
  2.7 1.4 %copy-done.2 = bf16[2816,256]{1,0:T(8,128)(2,1)S(1)} copy-done((bf16[2816,256]{1,0:T(8,128)(2,1)S(1)}, bf16[2816,256]{1,0:T(8,128)(2,1)}, u32[]{:S(2)}) %copy-start.2) | copy-done | bytes 1441816
  4.1 0.0 copy-start.3
  4.1 0.9 copy-done.3
  5.0 0.0 copy-start.4
  5.0 0.8 copy-done.4
  5.8 0.0 copy-start.5
  5.8 0.8 copy-done.5
  6.6 0.0 copy-start.6
  6.6 0.7 copy-done.6
  7.3 0.0 copy-start.7
  7.3 0.7 copy-done.7
  8.0 118.7 %ffn.1 = bf16[512,256]{1,0:T(8,128)(2,1)S(1)} custom-call(bf16[512,256]{1,0:T(8,128)(2,1)S(1)} %bitcast.5, f32[1,256]{1,0:T(1,128)S(1)} %bitcast.6, bf16[256,2816]{1,0:T(8,128)(2,1)S(1)} %copy-done, bf16[256,2816]{1,0:T(8,128)(2,1)S(1)} %copy-done.1, f32[3,2816]{1,0:T(4,128)S(1)} %copy-done.4, f32[3,2816]{1,0:T(4,128)S(1)} %copy-done.5, ...), custom_call_target="tpu_custom_call" | custom-call | tf_op jit(solution)/shard_map/ffn/pallas_call | solution.py:495
  126.7 0.7 copy.10
Async XLA Ops:
  0.0 1.4 %copy-start = (bf16[256,2816]{1,0:T(8,128)(2,1)S(1)}, bf16[256,2816]{1,0:T(8,128)(2,1)}, u32[]{:S(2)}) copy-start(bf16[256,2816]{1,0:T(8,128)(2,1)} %wg_ref.1) | copy-start | bytes 4325380
  1.4 1.4 %copy-start.1 = (bf16[256,2816]{1,0:T(8,128)(2,1)S(1)}, bf16[256,2816]{1,0:T(8,128)(2,1)}, u32[]{:S(2)}) copy-start(bf16[256,2816]{1,0:T(8,128)(2,1)} %wu_ref.1) | copy-start | bytes 4325380
  2.7 1.4 %copy-start.2 = (bf16[2816,256]{1,0:T(8,128)(2,1)S(1)}, bf16[2816,256]{1,0:T(8,128)(2,1)}, u32[]{:S(2)}) copy-start(bf16[2816,256]{1,0:T(8,128)(2,1)} %wd_hbm.1) | copy-start | bytes 4325380
  4.1 0.9 copy-start.3
  5.0 0.8 copy-start.4
  5.8 0.8 copy-start.5
  6.6 0.7 copy-start.6
  7.3 0.7 copy-start.7

commit v3 on v2

--- a/solution.py
+++ b/solution.py
@@ -16,9 +16,9 @@
 def _kernel(
     dim_full,
     nz,
-    tok_ref, pre_ref, wg_ref, wu_ref, cg_ref, cu_ref, wd_hbm, gain_ref,
+    tok_in, pre_in, wg_ref, wu_ref, cg_ref, cu_ref, wd_hbm, gain_in,
     out_ref,
-    xw_ref, sq_ref, ws_ref, wrows, wd_ref, taps_in, taps_ref,
+    tok_ref, pre_ref, gain_ref, xw_ref, sq_ref, ws_ref, wrows, wd_ref, taps_g, taps_u, taps_in, taps_ref,
     xfull, wfull, hfull, acc, part, psend, precv, sq_all, psq_own, psq_all,
     bshare, bfull, post_own, post_all, in_sem,
     xz_s, xz_r, y1_s, y1_r, y2_s, y2_r, wz_s, wz_r, wx_s, wx_r, wo_s, wo_r, wp_s, wp_r,
@@ -69,9 +69,16 @@
         pltpu.make_async_copy(wg_ref.at[own], wrows.at[0], in_sem.at[0]),
         pltpu.make_async_copy(wu_ref.at[own], wrows.at[1], in_sem.at[1]),
         pltpu.make_async_copy(wd_hbm, wd_ref, in_sem.at[2]),
+        pltpu.make_async_copy(tok_in, tok_ref, in_sem.at[3]),
+        pltpu.make_async_copy(pre_in, pre_ref, in_sem.at[4]),
+        pltpu.make_async_copy(gain_in, gain_ref, in_sem.at[5]),
+        pltpu.make_async_copy(cg_ref, taps_g, in_sem.at[6]),
+        pltpu.make_async_copy(cu_ref, taps_u, in_sem.at[7]),
     ]
-    for load in loads:
-        load.start()
+    for k in (3, 4, 0, 1, 5, 6, 7, 2):
+        loads[k].start()
+    loads[3].wait()
+    loads[4].wait()
     values = tok_ref[...].astype(F32)
     xw_ref[...] = (values * pre_ref[...]).astype(BF16)
     sq_ref[...] = jnp.sum(jnp.transpose(values * values, (1, 0)), axis=0, keepdims=True)
@@ -198,8 +205,10 @@
         sq_copy(zmod(z + d), z).start()
 
     acc[...] = jnp.zeros_like(acc)
-    taps_in[0:3] = cg_ref[...]
-    taps_in[3:6] = cu_ref[...]
+    loads[6].wait()
+    loads[7].wait()
+    taps_in[0:3] = taps_g[...]
+    taps_in[3:6] = taps_u[...]
     taps_in[6:8] = jnp.zeros((2, taps_in.shape[1]), F32)
     taps_ref[...] = jnp.transpose(taps_in[...], (1, 0))
 
@@ -314,6 +323,7 @@
         return lax.dot_general(w, hfull[b], (((0,), (0,)), ((), ())), preferred_element_type=F32)
 
     loads[2].wait()
+    loads[5].wait()
     part[...] = down(z)
 
     @pl.loop(1, half)
@@ -461,10 +471,15 @@
     vmem = pltpu.VMEM
     scratch = [
         vmem((positions, kb), BF16),
+        vmem((1, kb), F32),
+        vmem((1, kb), F32),
+        vmem((positions, kb), BF16),
         vmem((1, positions), F32),
         vmem((nz, rows, lanes), BF16),
         vmem((2, rows, ff), BF16),
         vmem((ff, kb), BF16),
+        vmem((3, ff), F32),
+        vmem((3, ff), F32),
         vmem((8, ff), F32),
         vmem((ff, 8), F32),
         vmem((nz, positions, kb), BF16),
@@ -481,7 +496,7 @@
         vmem((3, quarter, kb), BF16),
         vmem((1, quarter), F32),
         vmem((3, 1, quarter), F32),
-        dma((3,)),
+        dma((8,)),
         dma((2, nz)), dma((nz,)),
         dma((2, nz)), dma((2, nz)), dma((2, nz)), dma((2, nz)),
         dma((nz,)), dma((nz,)), dma((2, nz)), dma((2, nz)), dma((nz,)), dma((nz,)),
@@ -495,12 +510,12 @@
     out = pl.pallas_call(
         functools.partial(_kernel, dim_full, nz),
         out_shape=jax.ShapeDtypeStruct((positions, kb), BF16),
-        in_specs=[here, here, away, away, here, here, away, here],
+        in_specs=[away] * 8,
         out_specs=pl.BlockSpec(memory_space=pltpu.VMEM),
         scratch_shapes=scratch,
         name="ffn",
         compiler_params=pltpu.CompilerParams(
-            collective_id=0, has_side_effects=True, vmem_limit_bytes=48 * 1024 * 1024
+            collective_id=0, has_side_effects=True, vmem_limit_bytes=67043328
         ),
     )(tokens[0], pre_gain[None, :], w_gate, w_up, conv_gate, conv_up, w_down, post_gain[None, :])
     return out[None]

time: 129 us -> 122 us (0.946)
  local copies, waits for them, and re-layouts: 8.67 us -> 1.67 us
    unnamed x17 -> x1, local copies, waits for them, and re-layouts: 8.67 us -> 1.67 us
where the time goes in v3:
time: 122 us; the launch traced here: 121 us
  Pallas kernels  119 us (98%)
  local copies, waits for them, and re-layouts  1.67 us (1%)
    pallas_call x1, Pallas kernels, local(): pl.pallas_call(functools.partial(_kernel, dim_full, nz), out_shape=jax.Sh...  119 us

profile of v3, /device:TPU:6, one launch (start us, length us, event | category | flops | bytes accessed | tf_op | source)
XLA Modules:
  0.0 121.1 jit_solution(6377048626276276803)
XLA Ops:
  0.0 119.4 %ffn.1 = bf16[512,256]{1,0:T(8,128)(2,1)} custom-call(bf16[512,256]{1,0:T(8,128)(2,1)} %bitcast.5, f32[1,256]{1,0:T(1,128)} %bitcast.6, bf16[256,2816]{1,0:T(8,128)(2,1)} %wg_ref.1, bf16[256,2816]{1,0:T(8,128)(2,1)} %wu_ref.1, f32[3,2816]{1,0:T(4,128)} %cg_ref.1, f32[3,2816]{1,0:T(4,128)} %cu_ref.1, bf16[2816,256]{1,0:T(8,128)(2,1)} %wd_hbm.1, f32[1,256]{1,0:T(1,128)} %bitcast.7), custom_call_target="tpu_custom_call" | custom-call | tf_op jit(solution)/shard_map/ffn/pallas_call | solution.py:510
  119.5 1.7 %copy.10 = bf16[1,512,256]{2,1,0:T(8,128)(2,1)} copy(bf16[1,512,256]{2,1,0:T(8,128)(2,1)} %bitcast.4) | data formatting | bytes 524288

commit v4 on v3

--- a/solution.py
+++ b/solution.py
@@ -19,7 +19,7 @@
     tok_in, pre_in, wg_ref, wu_ref, cg_ref, cu_ref, wd_hbm, gain_in,
     out_ref,
     tok_ref, pre_ref, gain_ref, xw_ref, sq_ref, ws_ref, wrows, wd_ref, taps_g, taps_u, taps_in, taps_ref,
-    xfull, wfull, hfull, acc, part, psend, precv, sq_all, psq_own, psq_all,
+    xfull, wfull, hfull, acc, lin, part, psend, precv, sq_all, psq_own, psq_all,
     bshare, bfull, post_own, post_all, in_sem,
     xz_s, xz_r, y1_s, y1_r, y2_s, y2_r, wz_s, wz_r, wx_s, wx_r, wo_s, wo_r, wp_s, wp_r,
     sq_s, sq_r, hz_s, hz_r, ps_s, ps_r, pq_s, pq_r, mo_s, mo_r, po_s, po_r,
@@ -288,10 +288,17 @@
         sq_copy(src, src).wait_recv()
 
     scale = lax.rsqrt(jnp.sum(sq_all[...], axis=0) / dim_full + EPS)
-    lin = jnp.transpose(acc[...], (1, 0))
-    taps = taps_ref[pl.ds(pl.multiple_of(z * units, units), units), :]
-
-    def conv(field, base):
+    lin[...] = jnp.transpose(acc[...], (1, 0))
+    step_rows = -(-units // 64) * 16
+    cuts = [(r, min(step_rows, units - r)) for r in range(0, units, step_rows)]
+    subs = len(cuts)
+
+    def hz_copy(b, c, right):
+        ref = hfull.at[b, pl.ds(*cuts[c])]
+        return rcopy(ref, ref, hz_s.at[1 - right, b, c], hz_r.at[b, c],
+                     {"ra": z_right if right else z_left})
+
+    def conv(field, taps, base):
         lane = lax.broadcasted_iota(jnp.int32, field.shape, 1)
         before = jnp.where(lane == 0, 0.0, pltpu.roll(field, 1, 1))
         after = jnp.where(lane == tokens - 1, 0.0, pltpu.roll(field, tokens - 1, 1))
@@ -301,22 +308,29 @@
             + taps[:, base + 2 : base + 3] * after
         )
 
-    gate = conv(lin[:units] * scale, 0)
-    up = conv(lin[units : 2 * units] * scale, 3)
-    hidden = (jax.nn.gelu(gate, approximate=True) * up).astype(BF16)
-    hfull[z] = hidden
-    step_rows = -(-units // 64) * 16
-    cuts = [(r, min(step_rows, units - r)) for r in range(0, units, step_rows)]
-    subs = len(cuts)
-
-    def hz_copy(b, c, right):
-        ref = hfull.at[b, pl.ds(*cuts[c])]
-        return rcopy(ref, ref, hz_s.at[1 - right, b, c], hz_r.at[b, c],
-                     {"ra": z_right if right else z_left})
-
-    for c in range(subs):
+    for c, (r, count) in enumerate(cuts):
+        taps = taps_ref[pl.ds(pl.multiple_of(z * units + r, 16), count), :]
+        gate = conv(lin[r : r + count] * scale, taps, 0)
+        up = conv(lin[units + r : units + r + count] * scale, taps, 3)
+        hfull[z, r : r + count] = (jax.nn.gelu(gate, approximate=True) * up).astype(BF16)
         hz_copy(z, c, 1).start()
         hz_copy(z, c, 0).start()
+
+    def drain_first(b):
+        wx_copy(b, 1, dp).wait_send()
+        wx_copy(b, 0, dp).wait_send()
+        wo_copy(b, 1, x_left).wait_send()
+        for k in range(4):
+            wp_copy(b, k, dp).wait_send()
+
+        @pl.when(b != z)
+        def _():
+            y1_copy(b, 1, y).wait_send()
+            y1_copy(b, 0, y).wait_send()
+            y2_copy(b, 1, y_left).wait_send()
+            y2_copy(b, 0, y_right).wait_send()
+            wz_copy(b, z).wait_send()
+            sq_copy(b, z).wait_send()
 
     def down(b):
         w = wd_ref[pl.ds(pl.multiple_of(b * units, units), units), :]
@@ -346,6 +360,8 @@
                     hz_copy(bl, c, 0).start()
         part[...] += down(br)
         part[...] += down(bl)
+        drain_first(br)
+        drain_first(bl)
 
     far = zmod(z + half)
     for c in range(subs):
@@ -361,6 +377,30 @@
     for k, dest in enumerate((y_far, y_right, y_left)):
         psend[k] = part[:, quarter_cols(dest)].astype(BF16)
         ps_copy(k, dest).start()
+
+    for c in range(subs):
+        first = c < subs // 2
+
+        @pl.loop(0, half)
+        def _(t):
+            @pl.when(t < (half if first else half - 1))
+            def _():
+                hz_copy(zmod(z - t), c, 1).wait_send()
+
+            @pl.when(t < (half - 1 if first else half))
+            def _():
+                hz_copy(zmod(z + t), c, 0).wait_send()
+
+    @pl.loop(0, half)
+    def _(t):
+        xz_copy(zmod(z - t), 1).wait_send()
+
+        @pl.when(t < half - 1)
+        def _():
+            xz_copy(zmod(z + t), 0).wait_send()
+
+    drain_first(z)
+    drain_first(far)
     share = part[:, quarter_cols(y)]
     for k, dest in enumerate((y_far, y_right, y_left)):
         ps_copy(k, dest).wait_recv()
@@ -404,6 +444,13 @@
         col = jnp.transpose(jnp.broadcast_to(scale_row, (quarter, quarter)), (1, 0))[:, :1]
         base = RESIDUAL * tok_ref[q_rows(q), :].astype(F32)
         out_ref[q_rows(q), :] = (base + value * col).astype(BF16)
+
+    for k, dest in enumerate(peers):
+        ps_copy(k, dest).wait_send()
+
+    @pl.loop(1, nz)
+    def _(d):
+        pq_copy(zmod(z + d), z).wait_send()
 
     finish(y, branch, post)
     for k, source in enumerate((y_far, y_left, y_right)):
@@ -411,47 +458,7 @@
         po_copy(k, source).wait_recv()
         finish(source, bfull[k].astype(F32), post_all[k])
 
-    for c in range(subs):
-        first = c < subs // 2
-
-        @pl.loop(0, half)
-        def _(t):
-            @pl.when(t < (half if first else half - 1))
-            def _():
-                hz_copy(zmod(z - t), c, 1).wait_send()
-
-            @pl.when(t < (half - 1 if first else half))
-            def _():
-                hz_copy(zmod(z + t), c, 0).wait_send()
-
-    @pl.loop(0, half)
-    def _(t):
-        xz_copy(zmod(z - t), 1).wait_send()
-
-        @pl.when(t < half - 1)
-        def _():
-            xz_copy(zmod(z + t), 0).wait_send()
-
-    @pl.loop(0, nz)
-    def _(b):
-        @pl.when(b != z)
-        def _():
-            y1_copy(b, 1, y).wait_send()
-            y1_copy(b, 0, y).wait_send()
-            y2_copy(b, 1, y_left).wait_send()
-            y2_copy(b, 0, y_right).wait_send()
-            wz_copy(b, z).wait_send()
-            sq_copy(b, z).wait_send()
-            pq_copy(b, z).wait_send()
-
-        wx_copy(b, 1, dp).wait_send()
-        wx_copy(b, 0, dp).wait_send()
-        wo_copy(b, 1, x_left).wait_send()
-        for k in range(4):
-            wp_copy(b, k, dp).wait_send()
-
     for k, dest in enumerate(peers):
-        ps_copy(k, dest).wait_send()
         mo_copy(k, dest).wait_send()
         po_copy(k, dest).wait_send()
 
@@ -486,6 +493,7 @@
         vmem((nz, 8, rows, lanes), BF16),
         vmem((nz, units, positions), BF16),
         vmem((positions, lanes), F32),
+        vmem((lanes, positions), F32),
         vmem((kb, positions), F32),
         vmem((3, kb, quarter), BF16),
         vmem((3, kb, quarter), BF16),

time: 122 us -> 121 us (level)
    pallas_call x1, Pallas kernels: 119 us -> 118 us  [local(): pl.pallas_call(functools.partial(_kernel, dim_full, nz), out_shape=jax.Sh...]
where the time goes in v4:
time: 121 us; the launch traced here: 119 us
  Pallas kernels  118 us (98%)
  local copies, waits for them, and re-layouts  1.67 us (1%)
    pallas_call x1, Pallas kernels, local(): pl.pallas_call(functools.partial(_kernel, dim_full, nz), out_shape=jax.Sh...  118 us

profile of v4, /device:TPU:6, one launch (start us, length us, event | category | flops | bytes accessed | tf_op | source)
XLA Modules:
  0.0 119.5 jit_solution(10195660793778568123)
XLA Ops:
  0.0 117.8 %ffn.1 = bf16[512,256]{1,0:T(8,128)(2,1)} custom-call(bf16[512,256]{1,0:T(8,128)(2,1)} %bitcast.5, f32[1,256]{1,0:T(1,128)} %bitcast.6, bf16[256,2816]{1,0:T(8,128)(2,1)} %wg_ref.1, bf16[256,2816]{1,0:T(8,128)(2,1)} %wu_ref.1, f32[3,2816]{1,0:T(4,128)} %cg_ref.1, f32[3,2816]{1,0:T(4,128)} %cu_ref.1, bf16[2816,256]{1,0:T(8,128)(2,1)} %wd_hbm.1, f32[1,256]{1,0:T(1,128)} %bitcast.7), custom_call_target="tpu_custom_call" | custom-call | tf_op jit(solution)/shard_map/ffn/pallas_call | solution.py:518
  117.8 1.7 %copy.10 = bf16[1,512,256]{2,1,0:T(8,128)(2,1)} copy(bf16[1,512,256]{2,1,0:T(8,128)(2,1)} %bitcast.4) | data formatting | bytes 524288

commit v5 on v4

--- a/solution.py
+++ b/solution.py
@@ -22,7 +22,7 @@
     xfull, wfull, hfull, acc, lin, part, psend, precv, sq_all, psq_own, psq_all,
     bshare, bfull, post_own, post_all, in_sem,
     xz_s, xz_r, y1_s, y1_r, y2_s, y2_r, wz_s, wz_r, wx_s, wx_r, wo_s, wo_r, wp_s, wp_r,
-    sq_s, sq_r, hz_s, hz_r, ps_s, ps_r, pq_s, pq_r, mo_s, mo_r, po_s, po_r,
+    sq_s, sq_r, hz_s, hz_r, ps_s, ps_r, pq_s, pq_r, mo_s, mo_r, po_s, po_r, in_right, in_left,
 ):
     half = nz // 2
     z = lax.axis_index("ra")
@@ -55,10 +55,8 @@
 
     bar = pltpu.get_barrier_semaphore()
 
-    @pl.loop(1, nz)
-    def _(d):
-        pl.semaphore_signal(bar, inc=1, device_id={"ra": zmod(z + d)}, device_id_type=MESH)
-
+    for t in (z_right, z_left):
+        pl.semaphore_signal(bar, inc=1, device_id={"ra": t}, device_id_type=MESH)
     for t in (y_right, y_left, y_far):
         pl.semaphore_signal(bar, inc=1, device_id={"cb": t}, device_id_type=MESH)
     for t in (x_right, x_left, partner):
@@ -81,6 +79,135 @@
     loads[4].wait()
     values = tok_ref[...].astype(F32)
     xw_ref[...] = (values * pre_ref[...]).astype(BF16)
+    pl.semaphore_wait(bar, 8)
+
+    def relay(k):
+        @pl.when(k <= half)
+        def _():
+            pl.semaphore_signal(in_right, inc=1, device_id={"ra": z_right}, device_id_type=MESH)
+
+        @pl.when(k < half)
+        def _():
+            pl.semaphore_signal(in_left, inc=1, device_id={"ra": z_left}, device_id_type=MESH)
+
+    def heard(k):
+        @pl.when(k <= half)
+        def _():
+            pl.semaphore_wait(in_right, 1)
+
+        @pl.when(k < half)
+        def _():
+            pl.semaphore_wait(in_left, 1)
+
+        relay(k + 1)
+
+    relay(2)
+
+    def q_rows(q):
+        return pl.ds(pl.multiple_of(q * quarter, quarter), quarter)
+
+    def qh_rows(q, i):
+        return pl.ds(pl.multiple_of(q * quarter + i * qhalf, qhalf), qhalf)
+
+    def xz_copy(b, right, src=None):
+        dst = xfull.at[b, q_rows(y)]
+        return rcopy(dst if src is None else src, dst, xz_s.at[1 - right, b], xz_r.at[b],
+                     {"ra": z_right if right else z_left})
+
+    def y1_copy(b, right, q):
+        ref = xfull.at[b, q_rows(q)]
+        return rcopy(ref, ref, y1_s.at[1 - right, b], y1_r.at[1 - right, b],
+                     {"cb": y_right if right else y_left})
+
+    def y2_copy(b, right, q):
+        ref = xfull.at[b, qh_rows(q, 1 - right)]
+        return rcopy(ref, ref, y2_s.at[1 - right, b], y2_r.at[1 - right, b],
+                     {"cb": y_right if right else y_left})
+
+    def wz_copy(dest, source):
+        return rcopy(ws_ref.at[dest], wfull.at[source, dp], wz_s.at[dest], wz_r.at[source],
+                     {"ra": dest})
+
+    def wx_copy(b, right, share, src=None):
+        ref = wfull.at[b, share]
+        return rcopy(ref if src is None else src, ref, wx_s.at[1 - right, b], wx_r.at[1 - right, b],
+                     {"dp": x_right if right else x_left})
+
+    def wo_copy(b, right, share):
+        ref = wfull.at[b, share]
+        return rcopy(ref, ref, wo_s.at[b], wo_r.at[b], {"dp": x_right if right else x_left})
+
+    def wp_copy(b, k, share, src=None):
+        ref = wfull.at[b, share]
+        return rcopy(ref if src is None else src, ref, wp_s.at[k, b], wp_r.at[k, b], {"dp": partner})
+
+    def sq_copy(dest, source):
+        return rcopy(sq_ref, sq_all.at[source], sq_s.at[dest], sq_r.at[source], {"ra": dest})
+
+    def w_issue(d):
+        @pl.when(d <= half)
+        def _():
+            wz_copy(zmod(z + d), z).start()
+            sq_copy(zmod(z + d), z).start()
+
+        @pl.when(d < half)
+        def _():
+            wz_copy(zmod(z - d), z).start()
+            sq_copy(zmod(z - d), z).start()
+
+    def both(d, fn):
+        fn(zmod(z - d))
+
+        @pl.when((d > 0) & (d < half))
+        def _():
+            fn(zmod(z + d))
+
+    def w_arrive(b):
+        wz_copy(b, b).wait_recv()
+        wp_copy(b, 0, dp).start()
+        wx_copy(b, 1, dp).start()
+        wx_copy(b, 0, dp).start()
+
+    def w_side(b):
+        wx_copy(b, 1, x_left).wait_recv()
+        wx_copy(b, 0, x_right).wait_recv()
+        wp_copy(b, 1, x_left).start()
+        wp_copy(b, 2, x_right).start()
+
+        @pl.when(lax.rem(b, 2) == 0)
+        def _():
+            wo_copy(b, 1, x_left).start()
+
+        @pl.when(lax.rem(b, 2) == 1)
+        def _():
+            wo_copy(b, 0, x_right).start()
+
+    def w_far(b):
+        wo_copy(b, 1, x_far).wait_recv()
+        wp_copy(b, 3, x_far).start()
+
+    def w_last(b):
+        wp_copy(b, 0, partner).wait_recv()
+        wp_copy(b, 1, other(x_left)).wait_recv()
+        wp_copy(b, 2, other(x_right)).wait_recv()
+        wp_copy(b, 3, other(x_far)).wait_recv()
+
+    def x_first(b):
+        y1_copy(b, 1, y).start()
+        y1_copy(b, 0, y).start()
+
+    def x_second(b):
+        y1_copy(b, 1, y_left).wait_recv()
+        y2_copy(b, 1, y_left).start()
+        y1_copy(b, 0, y_right).wait_recv()
+        y2_copy(b, 0, y_right).start()
+
+    def x_third(b):
+        y2_copy(b, 1, y_far).wait_recv()
+        y2_copy(b, 0, y_far).wait_recv()
+
+    xz_copy(z, 1, xw_ref.at[q_rows(y)]).start()
+    xz_copy(z, 0, xw_ref.at[q_rows(y)]).start()
     sq_ref[...] = jnp.sum(jnp.transpose(values * values, (1, 0)), axis=0, keepdims=True)
     loads[0].wait()
     loads[1].wait()
@@ -91,118 +218,10 @@
     xfull[z] = xw_ref[...]
     wfull[z, dp] = ws_ref[z]
     sq_all[z] = sq_ref[...]
-    pl.semaphore_wait(bar, nz - 1 + 6)
-
-    def q_rows(q):
-        return pl.ds(pl.multiple_of(q * quarter, quarter), quarter)
-
-    def qh_rows(q, i):
-        return pl.ds(pl.multiple_of(q * quarter + i * qhalf, qhalf), qhalf)
-
-    def xz_copy(b, right, src=None):
-        dst = xfull.at[b, q_rows(y)]
-        return rcopy(dst if src is None else src, dst, xz_s.at[1 - right, b], xz_r.at[b],
-                     {"ra": z_right if right else z_left})
-
-    def y1_copy(b, right, q):
-        ref = xfull.at[b, q_rows(q)]
-        return rcopy(ref, ref, y1_s.at[1 - right, b], y1_r.at[1 - right, b],
-                     {"cb": y_right if right else y_left})
-
-    def y2_copy(b, right, q):
-        ref = xfull.at[b, qh_rows(q, 1 - right)]
-        return rcopy(ref, ref, y2_s.at[1 - right, b], y2_r.at[1 - right, b],
-                     {"cb": y_right if right else y_left})
-
-    def wz_copy(dest, source):
-        return rcopy(ws_ref.at[dest], wfull.at[source, dp], wz_s.at[dest], wz_r.at[source],
-                     {"ra": dest})
-
-    def wx_copy(b, right, share, src=None):
-        ref = wfull.at[b, share]
-        return rcopy(ref if src is None else src, ref, wx_s.at[1 - right, b], wx_r.at[1 - right, b],
-                     {"dp": x_right if right else x_left})
-
-    def wo_copy(b, right, share):
-        ref = wfull.at[b, share]
-        return rcopy(ref, ref, wo_s.at[b], wo_r.at[b], {"dp": x_right if right else x_left})
-
-    def wp_copy(b, k, share, src=None):
-        ref = wfull.at[b, share]
-        return rcopy(ref if src is None else src, ref, wp_s.at[k, b], wp_r.at[k, b], {"dp": partner})
-
-    def sq_copy(dest, source):
-        return rcopy(sq_ref, sq_all.at[source], sq_s.at[dest], sq_r.at[source], {"ra": dest})
-
-    def w_issue(d):
-        wz_copy(zmod(z + d), z).start()
-
-        @pl.when(d < half)
-        def _():
-            wz_copy(zmod(z - d), z).start()
-
-    def both(d, fn):
-        fn(zmod(z - d))
-
-        @pl.when((d > 0) & (d < half))
-        def _():
-            fn(zmod(z + d))
-
-    def w_arrive(b):
-        wz_copy(b, b).wait_recv()
-        wp_copy(b, 0, dp).start()
-        wx_copy(b, 1, dp).start()
-        wx_copy(b, 0, dp).start()
-
-    def w_side(b):
-        wx_copy(b, 1, x_left).wait_recv()
-        wx_copy(b, 0, x_right).wait_recv()
-        wp_copy(b, 1, x_left).start()
-        wp_copy(b, 2, x_right).start()
-
-        @pl.when(lax.rem(b, 2) == 0)
-        def _():
-            wo_copy(b, 1, x_left).start()
-
-        @pl.when(lax.rem(b, 2) == 1)
-        def _():
-            wo_copy(b, 0, x_right).start()
-
-    def w_far(b):
-        wo_copy(b, 1, x_far).wait_recv()
-        wp_copy(b, 3, x_far).start()
-
-    def w_last(b):
-        wp_copy(b, 0, partner).wait_recv()
-        wp_copy(b, 1, other(x_left)).wait_recv()
-        wp_copy(b, 2, other(x_right)).wait_recv()
-        wp_copy(b, 3, other(x_far)).wait_recv()
-
-    def x_first(b):
-        y1_copy(b, 1, y).start()
-        y1_copy(b, 0, y).start()
-
-    def x_second(b):
-        y1_copy(b, 1, y_left).wait_recv()
-        y2_copy(b, 1, y_left).start()
-        y1_copy(b, 0, y_right).wait_recv()
-        y2_copy(b, 0, y_right).start()
-
-    def x_third(b):
-        y2_copy(b, 1, y_far).wait_recv()
-        y2_copy(b, 0, y_far).wait_recv()
-
-    xz_copy(z, 1, xw_ref.at[q_rows(y)]).start()
-    xz_copy(z, 0, xw_ref.at[q_rows(y)]).start()
     w_issue(1)
-    w_issue(2)
     wp_copy(z, 0, dp, ws_ref.at[z]).start()
     wx_copy(z, 1, dp, ws_ref.at[z]).start()
     wx_copy(z, 0, dp, ws_ref.at[z]).start()
-
-    @pl.loop(1, nz)
-    def _(d):
-        sq_copy(zmod(z + d), z).start()
 
     acc[...] = jnp.zeros_like(acc)
     loads[6].wait()
@@ -250,13 +269,21 @@
 
                 x_first(bl)
 
-        @pl.when(s + 2 <= half)
+        heard(2 * s)
+
+        @pl.when(s <= 2)
+        def _():
+            w_issue(s + 1)
+
+        @pl.when(s >= 2)
         def _():
             w_issue(s + 2)
 
         @pl.when((s >= 2) & (s <= half + 1))
         def _():
             both(s - 1, x_second)
+
+        heard(2 * s + 1)
 
         with_first(s, w_arrive)
 
@@ -511,6 +538,7 @@
         dma((4, nz)), dma((4, nz)),
         dma((nz,)), dma((nz,)), dma((2, nz, subs)), dma((nz, subs)),
         dma((3,)), dma((3,)), dma((nz,)), dma((nz,)), dma((3,)), dma((3,)), dma((3,)), dma((3,)),
+        pltpu.SemaphoreType.REGULAR, pltpu.SemaphoreType.REGULAR,
     ]
 
     here = pl.BlockSpec(memory_space=pltpu.VMEM)

time: 121 us -> 118 us (0.975)
  Pallas kernels: 118 us -> 116 us
    pallas_call x1, Pallas kernels: 118 us -> 116 us  [local(): pl.pallas_call(functools.partial(_kernel, dim_full, nz), out_shape=jax.Sh...]
where the time goes in v5:
time: 118 us
  Pallas kernels  116 us (98%)
  local copies, waits for them, and re-layouts  1.67 us (1%)
    pallas_call x1, Pallas kernels, local(): pl.pallas_call(functools.partial(_kernel, dim_full, nz), out_shape=jax.Sh...  116 us

profile of v5, /device:TPU:6, one launch (start us, length us, event | category | flops | bytes accessed | tf_op | source)
XLA Modules:
  0.0 117.7 jit_solution(10230422941258523718)
XLA Ops:
  0.0 116.0 %ffn.1 = bf16[512,256]{1,0:T(8,128)(2,1)} custom-call(bf16[512,256]{1,0:T(8,128)(2,1)} %bitcast.5, f32[1,256]{1,0:T(1,128)} %bitcast.6, bf16[256,2816]{1,0:T(8,128)(2,1)} %wg_ref.1, bf16[256,2816]{1,0:T(8,128)(2,1)} %wu_ref.1, f32[3,2816]{1,0:T(4,128)} %cg_ref.1, f32[3,2816]{1,0:T(4,128)} %cu_ref.1, bf16[2816,256]{1,0:T(8,128)(2,1)} %wd_hbm.1, f32[1,256]{1,0:T(1,128)} %bitcast.7), custom_call_target="tpu_custom_call" | custom-call | tf_op jit(solution)/shard_map/ffn/pallas_call | solution.py:546
  116.0 1.7 %copy.10 = bf16[1,512,256]{2,1,0:T(8,128)(2,1)} copy(bf16[1,512,256]{2,1,0:T(8,128)(2,1)} %bitcast.4) | data formatting | bytes 524288

commit v6 on v5

--- a/solution.py
+++ b/solution.py
@@ -109,9 +109,9 @@
     def qh_rows(q, i):
         return pl.ds(pl.multiple_of(q * quarter + i * qhalf, qhalf), qhalf)
 
-    def xz_copy(b, right, src=None):
-        dst = xfull.at[b, q_rows(y)]
-        return rcopy(dst if src is None else src, dst, xz_s.at[1 - right, b], xz_r.at[b],
+    def xz_copy(b, i, right, src=None):
+        ref = (xfull.at[b] if src is None else src).at[qh_rows(y, i)]
+        return rcopy(ref, xfull.at[b, qh_rows(y, i)], xz_s.at[1 - right, b, i], xz_r.at[b, i],
                      {"ra": z_right if right else z_left})
 
     def y1_copy(b, right, q):
@@ -206,8 +206,9 @@
         y2_copy(b, 1, y_far).wait_recv()
         y2_copy(b, 0, y_far).wait_recv()
 
-    xz_copy(z, 1, xw_ref.at[q_rows(y)]).start()
-    xz_copy(z, 0, xw_ref.at[q_rows(y)]).start()
+    for i in range(2):
+        xz_copy(z, i, 1, xw_ref).start()
+        xz_copy(z, i, 0, xw_ref).start()
     sq_ref[...] = jnp.sum(jnp.transpose(values * values, (1, 0)), axis=0, keepdims=True)
     loads[0].wait()
     loads[1].wait()
@@ -250,22 +251,24 @@
         @pl.when(s <= half)
         def _():
             br = zmod(z - s)
-            xz_copy(br, 1).wait_recv()
-
-            @pl.when(s < half)
-            def _():
-                xz_copy(br, 1).start()
+            for i in range(2):
+                xz_copy(br, i, 1).wait_recv()
+
+                @pl.when(s < half)
+                def _():
+                    xz_copy(br, i, 1).start()
 
             x_first(br)
 
             @pl.when(s < half)
             def _():
                 bl = zmod(z + s)
-                xz_copy(bl, 0).wait_recv()
-
-                @pl.when(s < half - 1)
-                def _():
-                    xz_copy(bl, 0).start()
+                for i in range(2):
+                    xz_copy(bl, i, 0).wait_recv()
+
+                    @pl.when(s < half - 1)
+                    def _():
+                        xz_copy(bl, i, 0).start()
 
                 x_first(bl)
 
@@ -420,11 +423,13 @@
 
     @pl.loop(0, half)
     def _(t):
-        xz_copy(zmod(z - t), 1).wait_send()
+        for i in range(2):
+            xz_copy(zmod(z - t), i, 1).wait_send()
 
         @pl.when(t < half - 1)
         def _():
-            xz_copy(zmod(z + t), 0).wait_send()
+            for i in range(2):
+                xz_copy(zmod(z + t), i, 0).wait_send()
 
     drain_first(z)
     drain_first(far)
@@ -532,7 +537,7 @@
         vmem((1, quarter), F32),
         vmem((3, 1, quarter), F32),
         dma((8,)),
-        dma((2, nz)), dma((nz,)),
+        dma((2, nz, 2)), dma((nz, 2)),
         dma((2, nz)), dma((2, nz)), dma((2, nz)), dma((2, nz)),
         dma((nz,)), dma((nz,)), dma((2, nz)), dma((2, nz)), dma((nz,)), dma((nz,)),
         dma((4, nz)), dma((4, nz)),

time: 118 us -> 117 us (level)
  Pallas kernels: 116 us -> 114 us
    pallas_call x1, Pallas kernels: 116 us -> 114 us  [local(): pl.pallas_call(functools.partial(_kernel, dim_full, nz), out_shape=jax.Sh...]
where the time goes in v6:
time: 117 us; the launch traced here: 116 us
  Pallas kernels  114 us (97%)
  local copies, waits for them, and re-layouts  1.67 us (1%)
    pallas_call x1, Pallas kernels, local(): pl.pallas_call(functools.partial(_kernel, dim_full, nz), out_shape=jax.Sh...  114 us

profile of v6, /device:TPU:6, one launch (start us, length us, event | category | flops | bytes accessed | tf_op | source)
XLA Modules:
  0.0 115.8 jit_solution(4764983245952137228)
XLA Ops:
  0.0 114.1 %ffn.1 = bf16[512,256]{1,0:T(8,128)(2,1)} custom-call(bf16[512,256]{1,0:T(8,128)(2,1)} %bitcast.5, f32[1,256]{1,0:T(1,128)} %bitcast.6, bf16[256,2816]{1,0:T(8,128)(2,1)} %wg_ref.1, bf16[256,2816]{1,0:T(8,128)(2,1)} %wu_ref.1, f32[3,2816]{1,0:T(4,128)} %cg_ref.1, f32[3,2816]{1,0:T(4,128)} %cu_ref.1, bf16[2816,256]{1,0:T(8,128)(2,1)} %wd_hbm.1, f32[1,256]{1,0:T(1,128)} %bitcast.7), custom_call_target="tpu_custom_call" | custom-call | tf_op jit(solution)/shard_map/ffn/pallas_call | solution.py:551
  114.2 1.7 %copy.10 = bf16[1,512,256]{2,1,0:T(8,128)(2,1)} copy(bf16[1,512,256]{2,1,0:T(8,128)(2,1)} %bitcast.4) | data formatting | bytes 524288

commit v7 on v6

--- a/solution.py
+++ b/solution.py
@@ -390,8 +390,6 @@
                     hz_copy(bl, c, 0).start()
         part[...] += down(br)
         part[...] += down(bl)
-        drain_first(br)
-        drain_first(bl)
 
     far = zmod(z + half)
     for c in range(subs):
@@ -431,8 +429,6 @@
             for i in range(2):
                 xz_copy(zmod(z + t), i, 0).wait_send()
 
-    drain_first(z)
-    drain_first(far)
     share = part[:, quarter_cols(y)]
     for k, dest in enumerate((y_far, y_right, y_left)):
         ps_copy(k, dest).wait_recv()
@@ -461,6 +457,10 @@
     peers = (y_far, y_right, y_left)
     for k, dest in enumerate(peers):
         mo_copy(k, dest).start()
+
+    @pl.loop(0, nz)
+    def _(b):
+        drain_first(b)
 
     @pl.loop(1, nz)
     def _(d):

time: 117 us -> 117 us (level)
  no operation moved by 1% of the time
where the time goes in v7:
time: 117 us; the launch traced here: 116 us
  Pallas kernels  114 us (97%)
  local copies, waits for them, and re-layouts  1.67 us (1%)
    pallas_call x1, Pallas kernels, local(): pl.pallas_call(functools.partial(_kernel, dim_full, nz), out_shape=jax.Sh...  114 us

profile of v7, /device:TPU:6, one launch (start us, length us, event | category | flops | bytes accessed | tf_op | source)
XLA Modules:
  0.0 115.8 jit_solution(17778143096461474035)
XLA Ops:
  0.0 114.1 %ffn.1 = bf16[512,256]{1,0:T(8,128)(2,1)} custom-call(bf16[512,256]{1,0:T(8,128)(2,1)} %bitcast.5, f32[1,256]{1,0:T(1,128)} %bitcast.6, bf16[256,2816]{1,0:T(8,128)(2,1)} %wg_ref.1, bf16[256,2816]{1,0:T(8,128)(2,1)} %wu_ref.1, f32[3,2816]{1,0:T(4,128)} %cg_ref.1, f32[3,2816]{1,0:T(4,128)} %cu_ref.1, bf16[2816,256]{1,0:T(8,128)(2,1)} %wd_hbm.1, f32[1,256]{1,0:T(1,128)} %bitcast.7), custom_call_target="tpu_custom_call" | custom-call | tf_op jit(solution)/shard_map/ffn/pallas_call | solution.py:551
  114.2 1.7 %copy.10 = bf16[1,512,256]{2,1,0:T(8,128)(2,1)} copy(bf16[1,512,256]{2,1,0:T(8,128)(2,1)} %bitcast.4) | data formatting | bytes 524288
